TPU v7x, 512 devices: a whole 4x4x16 slice. The times are simulated.
512 devices in a mesh: sp: 64 (over z, y), tp: 8 (over x, core).
Axes of the slice: x: 4, y: 4, z: 16, core: 2. Of those that a mesh axis runs over, the one named last changes fastest.
Arguments:
- queries: bfloat16 [8192, 768], P('sp', 'tp'), may hold values from -6 to 6
- latents: bfloat16 [8192, 512], P('sp'), may hold values from -6 to 6
- rot_key: bfloat16 [8192, 32], P('sp'), may hold values from -6 to 6
- kv_weight: bfloat16 [512, 1024], P(None, 'tp'), may hold values from -0.25 to 0.25
- log_sums: float32 [8192, 8], P('sp', 'tp'), may hold values from 4 to 14, as said below
- outputs: bfloat16 [8192, 512], P('sp', 'tp'), may hold values from -4 to 4
- out_grad: bfloat16 [8192, 512], P('sp', 'tp'), may hold values from -384 to 384
Outputs:
- query_grad: bfloat16 [8192, 768], P('sp', 'tp')
- key_grad: bfloat16 [8192, 512], P('sp', 'tp')
- value_grad: bfloat16 [8192, 512], P('sp', 'tp')
- rot_grad: float32 [8192, 32], P('sp')
- weight_grad: float32 [512, 1024], P('sp', 'tp')
Inputs may be any that keep to these rules, and one draw needn't show every extreme that they name: `log_sums`: each value lies within one half of log(8192) + 0.5.
All inputs are finite; a program needn't handle non-finite values.
Results may differ from a plain program's by a relative error of at most 0.004.
The roundings to bfloat16 on the way count: a program that leaves them out, or rounds other values in their place, can miss the bound.
Values may be sent and summed in bfloat16 or wider, within the bound.
A program may use at most 64 MiB of HBM per device.

v0:
```python
import jax
import jax.numpy as jnp
from jax import lax
from jax.sharding import PartitionSpec as P

NOPE_DIM = 64
ROPE_DIM = 32
VALUE_DIM = 64


def in_one_piece(arrays, axis, dim, along):
    both = jnp.concatenate(arrays, axis=along)
    filled, at, outs = (lax.all_gather(both, axis, axis=dim, tiled=True), 0, [])
    for a in arrays:
        outs.append(lax.slice_in_dim(filled, at, at + a.shape[along], axis=along))
        at += a.shape[along]
    return tuple(outs)


def from_everyone(x, axis):
    copies = jnp.broadcast_to(x, (lax.axis_size(axis), *x.shape))
    return lax.all_to_all(copies, axis, split_axis=0, concat_axis=0, tiled=True)


def over_copies(x, axis):
    return from_everyone(x, axis).sum(axis=0)


def split_up(x, dim, length):
    before, after = (x.shape[:dim], x.shape[dim + 1 :])
    return jnp.moveaxis(x.reshape(*before, length, -1, *after), dim, 0)


def sent_and_summed(x, axis, dim):
    tiles = split_up(x, dim, lax.axis_size(axis))
    arrived = lax.all_to_all(tiles, axis, split_axis=0, concat_axis=0, tiled=True)
    return arrived.sum(axis=0)


def head_keys(joined_piece, rot_piece, head_count):
    piece_rows = joined_piece.shape[0]
    joined = joined_piece.reshape(piece_rows, head_count, NOPE_DIM + VALUE_DIM)
    rotary = rot_piece[:, None, :]
    return (jnp.concatenate([joined[:, :, :NOPE_DIM], rotary], axis=-1), joined[:, :, NOPE_DIM:])


def grad_scores(query_part, grad_part, key_full, values, log_part, delta_part):
    score_scale = (NOPE_DIM + ROPE_DIM) ** (-0.5)
    scores = (
        jnp.einsum("qhd,khd->hqk", query_part, key_full, preferred_element_type=jnp.float32)
        * score_scale
    )
    probs = jnp.exp(scores - log_part.T[:, :, None])
    dprob = jnp.einsum("qhd,khd->hqk", grad_part, values, preferred_element_type=jnp.float32)
    dscore = (probs * (dprob - delta_part.T[:, :, None])).astype(jnp.bfloat16)
    return (probs.astype(jnp.bfloat16), dscore)


def over_blocks(block_step, totals, pieces):
    piece_rows = pieces[0].shape[0]
    block_count = piece_rows // 1024
    stacked = tuple((member.reshape((block_count, 1024) + member.shape[1:]) for member in pieces))

    def scan_step(acc, item):
        block_index, parts = item
        return (block_step(acc, parts, block_index * 1024), None)

    totals, _ = lax.scan(scan_step, totals, (jnp.arange(block_count, dtype=jnp.int32), stacked))
    return totals


def per_device(queries, latents, rot_key, kv_weight, log_sums, outputs, out_grad):
    local_rows = queries.shape[0]
    head_count = log_sums.shape[1]
    head_dim = NOPE_DIM + ROPE_DIM
    score_scale = head_dim ** (-0.5)
    joined = jnp.dot(latents, kv_weight, preferred_element_type=jnp.float32).astype(jnp.bfloat16)
    own_keys, own_values = head_keys(joined, rot_key, head_count)
    own_queries = queries.reshape(local_rows, head_count, head_dim)
    own_grads = out_grad.reshape(local_rows, head_count, VALUE_DIM)
    row_delta = jnp.sum(
        outputs.astype(jnp.float32).reshape(local_rows, head_count, VALUE_DIM)
        * own_grads.astype(jnp.float32),
        axis=-1,
    )
    query_zero = jnp.zeros((local_rows, head_count, head_dim), jnp.float32)
    key_zero = jnp.zeros((local_rows, head_count, head_dim), jnp.float32)
    value_zero = jnp.zeros((local_rows, head_count, VALUE_DIM), jnp.float32)

    def query_step(query_total, pieces, start_row):
        keys_piece, values_piece = head_keys(pieces[0], pieces[1], head_count)
        probs_b, dscore = grad_scores(
            own_queries, own_grads, keys_piece, values_piece, log_sums, row_delta
        )
        return (
            query_total
            + jnp.einsum("hqk,khd->qhd", dscore, keys_piece, preferred_element_type=jnp.float32)
            * score_scale
        )

    query_total = over_blocks(query_step, query_zero, in_one_piece((joined, rot_key), "sp", 0, 1))
    all_logs, all_delta = in_one_piece((log_sums, row_delta), "sp", 0, 1)

    def key_step(totals, pieces, start_row):
        piece_rows = pieces[0].shape[0]
        query_part = pieces[0].reshape(piece_rows, head_count, head_dim)
        grad_part = pieces[1].reshape(piece_rows, head_count, VALUE_DIM)
        log_part = lax.dynamic_slice_in_dim(all_logs, start_row, piece_rows, 0)
        delta_part = lax.dynamic_slice_in_dim(all_delta, start_row, piece_rows, 0)
        probs_b, dscore = grad_scores(
            query_part, grad_part, own_keys, own_values, log_part, delta_part
        )
        key_next = (
            totals[0]
            + jnp.einsum("hqk,qhd->khd", dscore, query_part, preferred_element_type=jnp.float32)
            * score_scale
        )
        value_next = totals[1] + jnp.einsum(
            "hqk,qhd->khd", probs_b, grad_part, preferred_element_type=jnp.float32
        )
        return (key_next, value_next)

    key_total, value_total = over_blocks(
        key_step, (key_zero, value_zero), in_one_piece((queries, out_grad), "sp", 0, 1)
    )
    rot_grad = over_copies(jnp.sum(key_total[:, :, NOPE_DIM:], axis=1), "tp")
    key_grad = key_total[:, :, :NOPE_DIM].astype(jnp.bfloat16)
    value_grad = value_total.astype(jnp.bfloat16)
    stacked = jnp.concatenate([key_grad, value_grad], axis=-1).reshape(
        local_rows, head_count * (NOPE_DIM + VALUE_DIM)
    )
    weight_grad = sent_and_summed(
        lax.dot_general(
            latents, stacked, (((0,), (0,)), ((), ())), preferred_element_type=jnp.float32
        ),
        "sp",
        0,
    )
    query_grad = query_total.astype(jnp.bfloat16).reshape(local_rows, head_count * head_dim)
    return (
        query_grad,
        key_grad.reshape(local_rows, head_count * NOPE_DIM),
        value_grad.reshape(local_rows, head_count * VALUE_DIM),
        rot_grad,
        weight_grad,
    )


def solution(mesh):
    placed = (
        P("sp", "tp"),
        P("sp", None),
        P("sp", None),
        P(None, "tp"),
        P("sp", "tp"),
        P("sp", "tp"),
        P("sp", "tp"),
    )
    return jax.shard_map(
        per_device,
        mesh=mesh,
        in_specs=placed,
        out_specs=(P("sp", "tp"), P("sp", "tp"), P("sp", "tp"), P("sp", None), P("sp", "tp")),
        check_vma=False,
    )
```

profile of v0, /device:TPU:6, one launch (start us, length us, event | category | flops | bytes accessed | tf_op | source)
XLA Modules:
  0.0 337.4 jit_solution(9991707621675473649)
XLA Ops:
  7.2 1.4 pad_maximum_fusion.1
  9.8 1.3 pad_maximum_fusion
  12.6 88.7 %all_gather.11 = f32[8192,2]{0,1:T(2,128)S(1)} all-gather(f32[128,2]{0,1:T(2,128)S(1)} %pad_maximum_fusion.3), channel_id=1, replica_groups=mesh['sp'=64,'tp'=8] {'sp'}, dimensions={0}, use_global_device_ids=true | all-gather | bytes 66560 | tf_op jit(solution)/shard_map/all_gather | solution.py:13
  102.1 50.6 %all-gather.5.cloned.1.call-done = bf16[8192,160]{0,1:T(8,128)(2,1)} async-done(((bf16[128,160]{0,1:T(8,128)(2,1)}), bf16[8192,160]{0,1:T(8,128)(2,1)}) %all-gather.5.cloned.1.call-update) | async-done | bytes 2621456 | tf_op jit(solution)/shard_map/all_gather | solution.py:13
  152.7 2.7 slice.53
  155.4 3.2 copy.29
  158.6 1.8 copy.30
  160.4 33.0 %while.25 = (s32[]{:T(128)}, f32[128,1,96]{0,2,1:T(8,128)S(1)}, f32[128,1,64]{0,2,1:T(8,128)S(1)}, bf16[8,1024,96]{2,1,0:T(8,128)(2,1)S(1)}, bf16[128,1,96]{0,2,...) while((s32[]{:T(128)}, f32[128,1,96]{0,2,1:T(8,128)S(1)}, ...), condition=%wide.region_4.5_spmd.clone, body=%wide.region_3.4_spmd.clone.sunk | while | flops 84725760 | bytes 2852562 | solution.py:68
  161.9 1.4 fusion.80
  166.0 1.4 fusion.80
  167.4 1.2 fusion.81
  170.1 1.4 fusion.80
  174.2 1.4 fusion.80
  178.4 1.4 fusion.80
  182.5 1.4 fusion.80
  186.6 1.4 fusion.80
  190.7 1.4 fusion.80
  194.0 4.8 %all-to-all-start = ((f32[8,128,32]{1,2,0:T(8,128)}), f32[8,128,32]{1,2,0:T(8,128)S(1)}, u32[]{:S(2)}, u32[]{:S(2)}) async-start(f32[8,128,32]{1,2,0:T(8,128)} %broadcast_in_dim.14), calls=%async_computation | async-start | bytes 262144 | tf_op jit(solution)/shard_map/all_to_all | solution.py:22
  199.8 89.0 %all-gather.3.cloned.1.call-done = bf16[8192,160]{0,1:T(8,128)(2,1)} async-done(((bf16[128,160]{0,1:T(8,128)(2,1)}), bf16[8192,160]{0,1:T(8,128)(2,1)}) %all-gather.3.cloned.1.call-update) | async-done | bytes 2621456 | tf_op jit(solution)/shard_map/all_gather | solution.py:13
  288.9 1.6 slice-done
  290.5 2.4 copy.32
  292.9 1.7 copy.33
  294.6 10.2 %all-to-all-start.1 = ((f32[64,8,128]{2,1,0:T(8,128)}), f32[64,8,128]{2,1,0:T(8,128)S(1)}, u32[]{:S(2)}, u32[]{:S(2)}) async-start(f32[64,8,128]{2,1,0:T(8,128)} %bitcast.15), calls=%async_computation.1 | async-start | bytes 524288 | tf_op jit(solution)/shard_map/all_to_all | solution.py:36
  304.9 22.6 %while.24 = (s32[]{:T(128)}, f32[128,1,96]{0,2,1:T(8,128)S(1)}, bf16[8,1024,128]{2,1,0:T(8,128)(2,1)}, bf16[8,1024,32]{2,1,0:T(8,128)(2,1)}, bf16[128,1,96]{0,2,...) while((s32[]{:T(128)}, f32[128,1,96]{0,2,1:T(8,128)S(1)}, ...), condition=%wide.region_2.3_spmd.clone, body=%wide.region_1.2_spmd.clone.sunk | while | flops 68587520 | bytes 2303095 | solution.py:68
  (103 shorter events, 45.6 us)
Async XLA Ops:
  7.2 1.5 copy-start
  7.2 145.5 %all-gather.5.cloned.1.call-start = ((), (), s32[]{:S(2)}) async-start(), calls=%async_computation.3 | async-start | bytes 2662400 | tf_op jit(solution)/shard_map/all_gather | solution.py:13
  8.7 280.2 %all-gather.3.cloned.1.call-start = ((), (), s32[]{:S(2)}) async-start(), calls=%async_computation.2 | async-start | bytes 2662400 | tf_op jit(solution)/shard_map/all_gather | solution.py:13
  155.4 3.2 slice-start.2
  194.0 100.6 %all-to-all-start = ((f32[8,128,32]{1,2,0:T(8,128)}), f32[8,128,32]{1,2,0:T(8,128)S(1)}, u32[]{:S(2)}, u32[]{:S(2)}) async-start(f32[8,128,32]{1,2,0:T(8,128)} %broadcast_in_dim.14), calls=%async_computation | async-start | bytes 262144 | tf_op jit(solution)/shard_map/all_to_all | solution.py:22
  288.9 1.6 slice-start
  290.4 2.4 slice-start.1
  292.9 12.0 %copy-start.1 = (bf16[128,96]{0,1:T(8,128)(2,1)S(1)}, bf16[128,96]{0,1:T(8,128)(2,1)}, u32[]{:S(2)}) copy-start(bf16[128,96]{0,1:T(8,128)(2,1)} %param.11) | copy-start | bytes 73732
  292.9 12.0 %copy-start.2 = (bf16[128,64]{0,1:T(8,128)(2,1)S(1)}, bf16[128,64]{0,1:T(8,128)(2,1)}, u32[]{:S(2)}) copy-start(bf16[128,64]{0,1:T(8,128)(2,1)} %param.17) | copy-start | bytes 49156
  292.9 12.0 %copy-start.3 = (f32[128,1]{0,1:T(1,128)S(1)}, f32[128,1]{0,1:T(1,128)}, u32[]{:S(2)}) copy-start(f32[128,1]{0,1:T(1,128)} %param.15) | copy-start | bytes 1540
  294.6 35.3 %all-to-all-start.1 = ((f32[64,8,128]{2,1,0:T(8,128)}), f32[64,8,128]{2,1,0:T(8,128)S(1)}, u32[]{:S(2)}, u32[]{:S(2)}) async-start(f32[64,8,128]{2,1,0:T(8,128)} %bitcast.15), calls=%async_computation.1 | async-start | bytes 524288 | tf_op jit(solution)/shard_map/all_to_all | solution.py:36
Sparse Core Ops, SparseCore 0:
  10.9 141.7 all-gather.4
  155.6 133.2 all-gather.2
where the time goes:
time: 339 us; the launch traced here: 337 us
  waiting for transfers between devices  140 us (41%)
  blocking collectives  88.7 us (26%)
  local copies, waits for them, and re-layouts  36 us (11%)
  matrix products  30.5 us (9%)
  starting transfers between devices  15.1 us (4%)
  between operations  14.2 us (4%)
  other arithmetic  7.34 us (2%)
  loops' own time  5.98 us (2%)
    all_gather x2, waiting for transfers between devices, in_one_piece(): filled, at, outs = (lax.all_gather(both, axis, axis=dim, tiled=True), 0, [])  140 us
    all_gather x1, blocking collectives, in_one_piece(): filled, at, outs = (lax.all_gather(both, axis, axis=dim, tiled=True), 0, [])  88.7 us
    dot_general x8, matrix products, key_step(): jnp.einsum('hqk,qhd->khd', dscore, query_part, preferred_element_type=jnp...  11 us
    all_to_all x1, starting transfers between devices, sent_and_summed(): lax.all_to_all(tiles, axis, split_axis=0, concat_axis=0, tiled=True)  10.2 us
    dot_general x8, matrix products, key_step(): jnp.einsum('hqk,qhd->khd', probs_b, grad_part, preferred_element_type=jnp...  9.58 us
    slice x10, local copies, waits for them, and re-layouts, in_one_piece(): outs.append(lax.slice_in_dim(filled, at, at + a.shape[along], axis=along))  9.3 us
    broadcast_in_dim x8, local copies, waits for them, and re-layouts, head_keys(): rotary = rot_piece[:, None, :]  7.79 us
    reshape x8, local copies, waits for them, and re-layouts, head_keys(): joined = joined_piece.reshape(piece_rows, head_count, NOPE_DIM + VALUE_DIM)  7.77 us
  transfers between devices with their start and end apart: 4, of which 2 were waited for; matrix products, arithmetic and copies ran while one was open for 21% of the time, Pallas kernels for 0%

commit v1 on v0

v1 whole, which is shorter than its diff:
```python
import jax
import jax.numpy as jnp
from jax import lax
from jax.experimental import pallas as pl
from jax.experimental.pallas import tpu as pltpu
from jax.sharding import PartitionSpec as P

MESH = pl.DeviceIdType.MESH
F32 = jnp.float32
BF16 = jnp.bfloat16

NOPE = 64
ROPE = 32
VAL = 64
RANK = 512
ROWS = 128
NY = 4
NZ = 16
NTP = 8
PACK = 176
SCALE = (NOPE + ROPE) ** -0.5
LOG2E = 1.4426950408889634

Q_FAR = 0
Q_Y = 3
KV = 15
LAT = 18
DQ_Y = 21
DQ_Z = 33
DKV = 36
DROT = 39
W_Y = 42
W_Z = 45
ROT = 60
COPIES = 67


def three(x):
    hi = x.astype(BF16)
    rest = x - hi.astype(F32)
    mid = rest.astype(BF16)
    low = (rest - mid.astype(F32)).astype(BF16)
    return [hi.astype(F32), mid.astype(F32), low.astype(F32)]


def dot(a, b):
    return jnp.dot(a, b, preferred_element_type=F32)


def dot_nt(a, b):
    return lax.dot_general(a, b, (((1,), (1,)), ((), ())), preferred_element_type=F32)


def kernel(
    q_ref, lat_ref, rot_ref, w_ref, lse_ref, o_ref, do_ref,
    dq_ref, dk_ref, dv_ref, drot_ref, dw_ref,
    qbuf, kvbuf, kt, latt, mbuf, acc, dqp, dqr, dqs, dqz, dkvs, dkvr, rots, rotr, rotx, wsend, wrecv, wzs, wzr,
    ssem, rsem,
):
    sp = lax.axis_index("sp")
    tp = lax.axis_index("tp")
    z = sp // NY
    y = sp % NY
    odd = z % 2
    sign = 1 - 2 * odd

    def dev(dz, dy):
        return (((z + dz + NZ) % NZ) * NY + (y + dy + NY) % NY, tp)

    y_off = (0, 1, -1, 2)
    k_off = (0, 1, -1, 2 * sign)

    def copy(number, src, dst, device):
        return pltpu.make_async_remote_copy(
            src_ref=src, dst_ref=dst, send_sem=ssem.at[number], recv_sem=rsem.at[number],
            device_id=device, device_id_type=MESH,
        )

    barrier = pltpu.get_barrier_semaphore()
    greet = [dev(d, 0) for d in (1, -1, 2, -2, 4, -4)] + [dev(0, d) for d in (1, -1, 2)]
    greet += [(sp, (tp + k) % NTP) for k in range(1, NTP)]
    for device in greet:
        pl.semaphore_signal(barrier, inc=1, device_id=device, device_id_type=MESH)

    q_t = jnp.transpose(q_ref[...].astype(F32))
    do = do_ref[...].astype(F32)
    do_t = jnp.transpose(do)
    o_t = jnp.transpose(o_ref[...].astype(F32))
    delta = jnp.sum(o_t * do_t, axis=0, keepdims=True)
    lse = jnp.transpose(jnp.broadcast_to(lse_ref[...], (ROWS, ROWS)))[0:1] * (1.0 / SCALE)
    row = lax.broadcasted_iota(jnp.int32, (16, ROWS), 0)
    aux = jnp.zeros((16, ROWS), F32)
    for i, piece in enumerate(three(lse) + three(delta)):
        aux = jnp.where(row == i, jnp.broadcast_to(piece, (16, ROWS)), aux)
    qbuf[0, 0:64, :] = q_t[0:64].astype(BF16)
    qbuf[0, 64:128, :] = do_t.astype(BF16)
    qbuf[0, 128:160, :] = q_t[64:96].astype(BF16)
    qbuf[0, 160:176, :] = aux.astype(BF16)

    pl.semaphore_wait(barrier, len(greet))

    q_far = [
        copy(Q_FAR + 0, qbuf.at[0], qbuf.at[8], dev(-4, 0)),
        copy(Q_FAR + 1, qbuf.at[0], qbuf.at[4], dev(4, 0)),
        copy(Q_FAR + 2, qbuf.at[4 + 4 * odd], qbuf.at[12], dev(4 * sign, 0)),
    ]
    q_far[0].start()
    q_far[1].start()
    q_y = [
        [copy(Q_Y + 3 * t + u - 1, qbuf.at[4 * t], qbuf.at[4 * t + u], dev(0, y_off[u])) for u in (1, 2, 3)]
        for t in range(4)
    ]
    for c in q_y[0]:
        c.start()

    joined = dot(lat_ref[...], w_ref[...]).astype(BF16)
    kvbuf[0:ROWS, 0:128] = joined
    lane = lax.broadcasted_iota(jnp.int32, (ROWS, 128), 1)
    kvbuf[0:ROWS, 128:256] = jnp.where((lane >= ROPE) & (lane < ROPE + 6), -1.0, 0.0).astype(BF16)
    kvbuf[0:ROWS, 128 : 128 + ROPE] = rot_ref[...]

    def rows_of(s):
        return pl.ds(ROWS * s, ROWS)

    kv = [copy(KV + s - 1, kvbuf.at[rows_of(0)], kvbuf.at[rows_of(s)], dev(k_off[s], 0)) for s in (1, 2, 3)]
    for c in kv:
        c.start()
    latt[0] = jnp.transpose(lat_ref[...].astype(F32)).astype(BF16)
    lat = [copy(LAT + s - 1, latt.at[0], latt.at[s], dev(k_off[s], 0)) for s in (1, 2, 3)]
    for c in lat:
        c.start()

    mbuf[...] = jnp.zeros_like(mbuf)
    acc[...] = jnp.zeros_like(acc)

    for c in kv:
        c.wait_recv()
    kt[0:64, :] = jnp.transpose(kvbuf[:, 0:128].astype(F32))[0:64].astype(BF16)
    kt[64:96, :] = jnp.transpose(kvbuf[:, 128:256].astype(F32))[0:32].astype(BF16)

    def process(slot):
        mbuf[0:64, 0:128] = qbuf[slot, 0:64, :]
        mbuf[64:128, 128:256] = qbuf[slot, 64:128, :]
        mbuf[128:160, 0:128] = qbuf[slot, 128:160, :]
        extra = qbuf[slot, 160:176, :].astype(F32)
        mbuf[160:176, 0:128] = jnp.where(row < 3, extra, 0.0).astype(BF16)
        mbuf[160:176, 128:256] = jnp.where(row >= 3, extra, 0.0).astype(BF16)
        m = mbuf[...]
        total = jnp.zeros((96, ROWS), F32)
        for c in range(2):
            rows = pl.ds(256 * c, 256)
            both = dot(kvbuf[rows, :], m)
            probs = jnp.exp2(both[:, 0:128] * (SCALE * LOG2E))
            ds = (probs * both[:, 128:256]).astype(BF16)
            acc[rows, :] += dot_nt(jnp.concatenate([ds, probs.astype(BF16)], axis=1), m)
            total = total + dot(kt[:, 256 * c : 256 * c + 256], ds)
        dqp[slot] = total

    def dq_y(t, u, device):
        return copy(DQ_Y + 3 * t + u - 1, dqp.at[4 * t + u], dqr.at[3 * t + u - 1], device)

    def back(u):
        return dev(0, jnp.where(u == 1, -1, jnp.where(u == 2, 1, 2)))

    def steps(t, first):
        def step(u, carry):
            copy(Q_Y + 3 * t + u - 1, qbuf.at[4 * t], qbuf.at[4 * t + u], dev(0, 1)).wait_recv()
            process(4 * t + u)
            dq_y(t, u, back(u)).start()
            return carry

        if first:
            process(4 * t)
        lax.fori_loop(1, 4, step, 0)

    q_far[0].wait_recv()
    q_far[1].wait_recv()
    q_far[2].start()
    for t in (1, 2):
        for c in q_y[t]:
            c.start()
    steps(0, True)
    process(4)
    process(8)
    q_far[2].wait_recv()
    for c in q_y[3]:
        c.start()
    steps(1, False)
    steps(2, False)
    steps(3, True)

    lane_scale = jnp.where(lane < NOPE, SCALE, 1.0)
    for c in lat:
        c.wait_recv()
    wpart = jnp.zeros((RANK, 128), F32)
    dkv = []
    for s in (1, 2, 3, 0):
        main = acc[ROWS * s : ROWS * (s + 1), 0:128] * lane_scale
        dkvs[s] = main
        rots[s] = jnp.transpose(acc[ROWS * s : ROWS * (s + 1), 128:256])[0:ROPE] * SCALE
        if s:
            owner = dev(-k_off[s], 0)
            dkv.append(copy(DKV + s - 1, dkvs.at[s], dkvr.at[s - 1], owner))
            dkv.append(copy(DROT + s - 1, rots.at[s], rotr.at[s - 1], owner))
            dkv[-2].start()
            dkv[-1].start()
        hi = main.astype(BF16)
        low = (main - hi.astype(F32)).astype(BF16)
        wpart = wpart + dot(latt[s], hi) + dot(latt[s], low)
    wpart = wpart.reshape(NZ, NY, 8, 128)
    for v in range(NY):
        wsend[v] = wpart[:, v]
    w_y = []
    for u in (1, 2, 3):
        w_y.append(copy(W_Y + u - 1, wsend.at[(y + y_off[u] + NY) % NY], wrecv.at[u - 1], dev(0, y_off[u])))
        w_y[-1].start()

    def dq_sum(t):
        for u in (1, 2, 3):
            dq_y(t, u, dev(0, 1)).wait_recv()
        dqs[t] = dqp[4 * t] + dqr[3 * t] + dqr[3 * t + 1] + dqr[3 * t + 2]

    for t in (3, 1, 2, 0):
        dq_sum(t)
        if t == 3:
            dq_relay = copy(DQ_Z, dqs.at[3], dqz.at[0], dev(4 * sign, 0))
            dq_relay.start()
    dq_plain = copy(DQ_Z + 1, dqs.at[1 + odd], dqz.at[1], dev(-4 * sign, 0))
    dq_plain.start()

    for c in w_y:
        c.wait_recv()
    wzs[...] = wsend[y] + wrecv[0] + wrecv[1] + wrecv[2]
    w_z = []
    for d in range(1, NZ):
        w_z.append(copy(W_Z + d - 1, wzs.at[(z + d) % NZ], wzr.at[d - 1], dev(d, 0)))
        w_z[-1].start()

    for c in dkv:
        c.wait_recv()
    own = dkvs[0] + dkvr[0] + dkvr[1] + dkvr[2]
    rotx[tp] = rots[0] + rotr[0] + rotr[1] + rotr[2]
    rot = []
    for k in range(1, NTP):
        rot.append(copy(ROT + k - 1, rotx.at[tp], rotx.at[tp], (sp, (tp + k) % NTP)))
        rot[-1].start()
    own = own.astype(BF16)
    dk_ref[...] = own[:, 0:NOPE]
    dv_ref[...] = own[:, NOPE:128]

    dq_relay.wait_recv()
    dqs[2 - odd] = dqs[2 - odd] + dqz[0]
    dq_last = copy(DQ_Z + 2, dqs.at[2 - odd], dqz.at[2], dev(4 * sign, 0))
    dq_last.start()

    for k in range(1, NTP):
        rot[k - 1].wait_recv()
    total = rotx[0]
    for k in range(1, NTP):
        total = total + rotx[k]
    drot_ref[...] = jnp.transpose(jnp.concatenate([total, jnp.zeros((96, ROWS), F32)], axis=0))[:, 0:ROPE]

    for c in w_z:
        c.wait_recv()
    wsum = wzs[z]
    for d in range(1, NZ):
        wsum = wsum + wzr[d - 1]
    dw_ref[...] = wsum

    dq_plain.wait_recv()
    dq_last.wait_recv()
    dq_total = (dqs[0] + dqz[1] + dqz[2]) * SCALE
    dq_total = jnp.transpose(jnp.concatenate([dq_total, jnp.zeros((32, ROWS), F32)], axis=0))
    dq_ref[...] = dq_total[:, 0:96].astype(BF16)

    for c in q_far + kv + lat + dkv + w_y + w_z + rot + [dq_relay, dq_plain, dq_last]:
        c.wait_send()
    for t in range(4):
        for c in q_y[t]:
            c.wait_send()
        for u in (1, 2, 3):
            dq_y(t, u, dev(0, 1)).wait_send()


def per_device(*arrays):
    vmem = pl.BlockSpec(memory_space=pltpu.VMEM)
    shape = jax.ShapeDtypeStruct
    return pl.pallas_call(
        kernel,
        out_shape=(
            shape((ROWS, NOPE + ROPE), BF16),
            shape((ROWS, NOPE), BF16),
            shape((ROWS, VAL), BF16),
            shape((ROWS, ROPE), F32),
            shape((8, 128), F32),
        ),
        in_specs=[vmem] * 7,
        out_specs=(vmem,) * 5,
        scratch_shapes=[
            pltpu.VMEM((16, PACK, ROWS), BF16),
            pltpu.VMEM((4 * ROWS, 256), BF16),
            pltpu.VMEM((96, 4 * ROWS), BF16),
            pltpu.VMEM((4, RANK, ROWS), BF16),
            pltpu.VMEM((256, 256), BF16),
            pltpu.VMEM((4 * ROWS, 256), F32),
            pltpu.VMEM((16, 96, ROWS), F32),
            pltpu.VMEM((12, 96, ROWS), F32),
            pltpu.VMEM((4, 96, ROWS), F32),
            pltpu.VMEM((3, 96, ROWS), F32),
            pltpu.VMEM((4, ROWS, 128), F32),
            pltpu.VMEM((3, ROWS, 128), F32),
            pltpu.VMEM((4, ROPE, ROWS), F32),
            pltpu.VMEM((3, ROPE, ROWS), F32),
            pltpu.VMEM((NTP, ROPE, ROWS), F32),
            pltpu.VMEM((NY, NZ, 8, 128), F32),
            pltpu.VMEM((3, NZ, 8, 128), F32),
            pltpu.VMEM((NZ, 8, 128), F32),
            pltpu.VMEM((NZ - 1, 8, 128), F32),
            pltpu.SemaphoreType.DMA((COPIES,)),
            pltpu.SemaphoreType.DMA((COPIES,)),
        ],
        compiler_params=pltpu.CompilerParams(collective_id=0, has_side_effects=True),
    )(*arrays)


def solution(mesh):
    placed = (
        P("sp", "tp"),
        P("sp", None),
        P("sp", None),
        P(None, "tp"),
        P("sp", "tp"),
        P("sp", "tp"),
        P("sp", "tp"),
    )
    return jax.shard_map(
        per_device,
        mesh=mesh,
        in_specs=placed,
        out_specs=(P("sp", "tp"), P("sp", "tp"), P("sp", "tp"), P("sp", None), P("sp", "tp")),
        check_vma=False,
    )
```

time: 339 us -> 67.9 us (0.20)
  waiting for transfers between devices: 140 us -> 0 us
  blocking collectives: 88.7 us -> 0 us
  Pallas kernels: 0 us -> 57.5 us
  matrix products: 30.5 us -> 0 us
  local copies, waits for them, and re-layouts: 36 us -> 9.25 us
  starting transfers between devices: 15.1 us -> 0 us
  between operations: 14.2 us -> 0.67 us
  other arithmetic: 7.34 us -> 0 us
  loops' own time: 5.98 us -> 0 us
    all_gather x2 -> x0, waiting for transfers between devices: 140 us -> none  [in_one_piece(): filled, at, outs = (lax.all_gather(both, axis, axis=dim, tiled=True), 0, [])]
    all_gather x1 -> x0, blocking collectives: 88.7 us -> none  [in_one_piece(): filled, at, outs = (lax.all_gather(both, axis, axis=dim, tiled=True), 0, [])]
    pallas_call x0 -> x1, Pallas kernels: none -> 57.5 us  [per_device(): pl.pallas_call(kernel, out_shape=(shape((ROWS, NOPE + ROPE), BF16), shape...]
    dot_general x42 -> x0, matrix products: 30.5 us -> none  [the longest x8 11 us: key_step(): jnp.einsum('hqk,qhd->khd', dscore, query_part, preferred_element_type=jnp...]
    all_to_all x2 -> x0, starting transfers between devices: 15 us -> none  [the longest x1 10.2 us: sent_and_summed(): lax.all_to_all(tiles, axis, split_axis=0, concat_axis=0, tiled=True)]
    slice x12 -> x0, local copies, waits for them, and re-layouts: 9.31 us -> none  [the longest x10 9.3 us: in_one_piece(): outs.append(lax.slice_in_dim(filled, at, at + a.shape[along], axis=along))]
    broadcast_in_dim x9 -> x0, local copies, waits for them, and re-layouts: 8.45 us -> none  [the longest x8 7.79 us: head_keys(): rotary = rot_piece[:, None, :]]
    reshape x9 -> x0, local copies, waits for them, and re-layouts: 8.38 us -> none  [the longest x8 7.77 us: head_keys(): joined = joined_piece.reshape(piece_rows, head_count, NOPE_DIM + VALUE_DIM)]
  transfers between devices with their start and end apart: 4 -> 0, of which waited for: 2 -> 0; matrix products, arithmetic and copies ran while one was open for 21% -> 0% of each run, Pallas kernels for 0% -> 0%
where the time goes in v1:
time: 67.9 us; the launch traced here: 67.4 us
  Pallas kernels  57.5 us (85%)
  local copies, waits for them, and re-layouts  9.25 us (14%)
    pallas_call x1, Pallas kernels, per_device(): pl.pallas_call(kernel, out_shape=(shape((ROWS, NOPE + ROPE), BF16), shape...  57.5 us
    unnamed x20, local copies, waits for them, and re-layouts  4.93 us
    pallas_call x4, local copies, waits for them, and re-layouts, per_device(): pl.pallas_call(kernel, out_shape=(shape((ROWS, NOPE + ROPE), BF16), shape...  4.32 us

profile of v1, /device:TPU:6, one launch (start us, length us, event | category | flops | bytes accessed | tf_op | source)
XLA Modules:
  0.0 67.4 jit_solution(3482087389494365829)
XLA Ops:
  0.6 0.0 copy-start.4
  0.6 1.4 %copy.12.q_ref = bf16[128,96]{1,0:T(8,128)(2,1)} copy(bf16[128,96]{0,1:T(8,128)(2,1)} %param.7) | data formatting | bytes 49152 | tf_op args[0]
  2.1 0.0 copy-done.4
  2.1 0.0 copy-start.2
  2.1 0.7 %copy.13.rot_ref = bf16[128,32]{1,0:T(8,128)(2,1)} copy(bf16[128,32]{0,1:T(8,128)(2,1)S(1)} %copy-done.4) | data formatting | bytes 16384 | tf_op args[2]
  2.8 0.0 copy-done.2
  2.8 0.0 copy-start.3
  2.8 0.7 %copy.15.o_ref = bf16[128,64]{1,0:T(8,128)(2,1)} copy(bf16[128,64]{0,1:T(8,128)(2,1)S(1)} %copy-done.2) | data formatting | bytes 32768 | tf_op args[5]
  3.5 0.0 copy-done.3
  3.5 0.7 %copy.16.do_ref = bf16[128,64]{1,0:T(8,128)(2,1)} copy(bf16[128,64]{0,1:T(8,128)(2,1)S(1)} %copy-done.3) | data formatting | bytes 32768 | tf_op args[6]
  4.2 0.0 copy-done.6
  4.2 0.7 %copy.14.lse_ref = f32[128,1]{1,0:T(8,128)} copy(f32[128,1]{0,1:T(1,128)S(1)} %copy-done.6) | data formatting | bytes 1024 | tf_op args[4]
  5.0 57.5 %shard_map.110 = (bf16[128,96]{1,0:T(8,128)(2,1)}, bf16[128,64]{1,0:T(8,128)(2,1)}, bf16[128,64]{1,0:T(8,128)(2,1)}, f32[128,32]{1,0:T(8,128)}, f32[8,128]{1,0:T(8,128)}) custom-call(bf16[128,96]{1,0:T(8,128)(2,1)} %copy.12.q_ref, bf16[128,512]{1,0:T(8,128)(2,1)} %lat_ref.1, bf16[128,32]{1,0:T(8,128)(2,1)} %copy.13.rot_ref, bf16[512,128]{1,0:T(8,128)(2,1)} %w_ref.1, ...), custom_call_target="tpu_custom_call" | custom-call | tf_op jit(solution)/shard_map/pallas_call | solution.py:288
  62.5 0.0 copy-start
  62.5 1.5 %copy.17 = bf16[128,96]{0,1:T(8,128)(2,1)} copy(bf16[128,96]{1,0:T(8,128)(2,1)} %get-tuple-element.5) | data formatting | bytes 49152 | tf_op jit(solution)/shard_map/pallas_call | solution.py:288
  64.0 0.0 copy-start.1
  64.0 1.5 %copy.18 = bf16[128,64]{0,1:T(8,128)(2,1)} copy(bf16[128,64]{1,0:T(8,128)(2,1)} %get-tuple-element.6) | data formatting | bytes 32768 | tf_op jit(solution)/shard_map/pallas_call | solution.py:288
  65.5 0.0 copy-done.1
  65.5 0.7 %copy.19 = bf16[128,64]{0,1:T(8,128)(2,1)} copy(bf16[128,64]{1,0:T(8,128)(2,1)S(1)} %copy-done.1) | data formatting | bytes 32768 | tf_op jit(solution)/shard_map/pallas_call | solution.py:288
  66.2 0.0 copy-done
  66.2 0.0 copy-start.5
  66.2 0.7 %copy.20 = f32[128,32]{0,1:T(8,128)} copy(f32[128,32]{1,0:T(8,128)S(1)} %copy-done) | data formatting | bytes 32768 | tf_op jit(solution)/shard_map/pallas_call | solution.py:288
  66.8 0.0 copy-done.5
  66.9 0.6 copy.22
  (1 shorter events, 0.0 us)
Async XLA Ops:
  0.6 1.5 %copy-start.4 = (bf16[128,32]{0,1:T(8,128)(2,1)S(1)}, bf16[128,32]{0,1:T(8,128)(2,1)}, u32[]{:S(2)}) copy-start(bf16[128,32]{0,1:T(8,128)(2,1)} %param.9) | copy-start | bytes 24580
  2.1 0.7 %copy-start.2 = (bf16[128,64]{0,1:T(8,128)(2,1)S(1)}, bf16[128,64]{0,1:T(8,128)(2,1)}, u32[]{:S(2)}) copy-start(bf16[128,64]{0,1:T(8,128)(2,1)} %param.12) | copy-start | bytes 49156
  2.8 0.7 %copy-start.3 = (bf16[128,64]{0,1:T(8,128)(2,1)S(1)}, bf16[128,64]{0,1:T(8,128)(2,1)}, u32[]{:S(2)}) copy-start(bf16[128,64]{0,1:T(8,128)(2,1)} %param.13) | copy-start | bytes 49156
  3.5 0.7 %copy-start.6 = (f32[128,1]{0,1:T(1,128)S(1)}, f32[128,1]{0,1:T(1,128)}, u32[]{:S(2)}) copy-start(f32[128,1]{0,1:T(1,128)} %param.11) | copy-start | bytes 1540
  62.5 3.7 %copy-start = (f32[128,32]{1,0:T(8,128)S(1)}, f32[128,32]{1,0:T(8,128)}, u32[]{:S(2)}) copy-start(f32[128,32]{1,0:T(8,128)} %get-tuple-element.8) | copy-start | bytes 49156
  64.0 1.5 %copy-start.1 = (bf16[128,64]{1,0:T(8,128)(2,1)S(1)}, bf16[128,64]{1,0:T(8,128)(2,1)}, u32[]{:S(2)}) copy-start(bf16[128,64]{1,0:T(8,128)(2,1)} %get-tuple-element.7) | copy-start | bytes 49156
  66.2 0.7 %copy-start.5 = (f32[8,128]{1,0:T(8,128)S(1)}, f32[8,128]{1,0:T(8,128)}, u32[]{:S(2)}) copy-start(f32[8,128]{1,0:T(8,128)} %get-tuple-element.19) | copy-start | bytes 12292

commit v2 on v1

--- a/solution.py
+++ b/solution.py
@@ -82,19 +82,15 @@
     for device in greet:
         pl.semaphore_signal(barrier, inc=1, device_id=device, device_id_type=MESH)
 
-    q_t = jnp.transpose(q_ref[...].astype(F32))
-    do = do_ref[...].astype(F32)
-    do_t = jnp.transpose(do)
-    o_t = jnp.transpose(o_ref[...].astype(F32))
-    delta = jnp.sum(o_t * do_t, axis=0, keepdims=True)
-    lse = jnp.transpose(jnp.broadcast_to(lse_ref[...], (ROWS, ROWS)))[0:1] * (1.0 / SCALE)
+    delta = jnp.sum(o_ref[...].astype(F32) * do_ref[...].astype(F32), axis=0, keepdims=True)
+    lse = lse_ref[...] * (1.0 / SCALE)
     row = lax.broadcasted_iota(jnp.int32, (16, ROWS), 0)
     aux = jnp.zeros((16, ROWS), F32)
     for i, piece in enumerate(three(lse) + three(delta)):
         aux = jnp.where(row == i, jnp.broadcast_to(piece, (16, ROWS)), aux)
-    qbuf[0, 0:64, :] = q_t[0:64].astype(BF16)
-    qbuf[0, 64:128, :] = do_t.astype(BF16)
-    qbuf[0, 128:160, :] = q_t[64:96].astype(BF16)
+    qbuf[0, 0:64, :] = q_ref[0:64, :]
+    qbuf[0, 64:128, :] = do_ref[...]
+    qbuf[0, 128:160, :] = q_ref[64:96, :]
     qbuf[0, 160:176, :] = aux.astype(BF16)
 
     pl.semaphore_wait(barrier, len(greet))
@@ -116,8 +112,9 @@
     joined = dot(lat_ref[...], w_ref[...]).astype(BF16)
     kvbuf[0:ROWS, 0:128] = joined
     lane = lax.broadcasted_iota(jnp.int32, (ROWS, 128), 1)
-    kvbuf[0:ROWS, 128:256] = jnp.where((lane >= ROPE) & (lane < ROPE + 6), -1.0, 0.0).astype(BF16)
-    kvbuf[0:ROWS, 128 : 128 + ROPE] = rot_ref[...]
+    rot_rows = jnp.concatenate([rot_ref[...].astype(F32), jnp.zeros((ROWS - ROPE, ROWS), F32)], axis=0)
+    marks = jnp.where((lane >= ROPE) & (lane < ROPE + 6), -1.0, 0.0)
+    kvbuf[0:ROWS, 128:256] = (jnp.transpose(rot_rows) + marks).astype(BF16)
 
     def rows_of(s):
         return pl.ds(ROWS * s, ROWS)
@@ -244,9 +241,9 @@
     for k in range(1, NTP):
         rot.append(copy(ROT + k - 1, rotx.at[tp], rotx.at[tp], (sp, (tp + k) % NTP)))
         rot[-1].start()
-    own = own.astype(BF16)
-    dk_ref[...] = own[:, 0:NOPE]
-    dv_ref[...] = own[:, NOPE:128]
+    own = jnp.transpose(own).astype(BF16)
+    dk_ref[...] = own[0:NOPE]
+    dv_ref[...] = own[NOPE:128]
 
     dq_relay.wait_recv()
     dqs[2 - odd] = dqs[2 - odd] + dqz[0]
@@ -258,7 +255,7 @@
     total = rotx[0]
     for k in range(1, NTP):
         total = total + rotx[k]
-    drot_ref[...] = jnp.transpose(jnp.concatenate([total, jnp.zeros((96, ROWS), F32)], axis=0))[:, 0:ROPE]
+    drot_ref[...] = total
 
     for c in w_z:
         c.wait_recv()
@@ -269,9 +266,7 @@
 
     dq_plain.wait_recv()
     dq_last.wait_recv()
-    dq_total = (dqs[0] + dqz[1] + dqz[2]) * SCALE
-    dq_total = jnp.transpose(jnp.concatenate([dq_total, jnp.zeros((32, ROWS), F32)], axis=0))
-    dq_ref[...] = dq_total[:, 0:96].astype(BF16)
+    dq_ref[...] = ((dqs[0] + dqz[1] + dqz[2]) * SCALE).astype(BF16)
 
     for c in q_far + kv + lat + dkv + w_y + w_z + rot + [dq_relay, dq_plain, dq_last]:
         c.wait_send()
@@ -282,16 +277,16 @@
             dq_y(t, u, dev(0, 1)).wait_send()
 
 
-def per_device(*arrays):
+def per_device(queries, latents, rot_key, kv_weight, log_sums, outputs, out_grad):
     vmem = pl.BlockSpec(memory_space=pltpu.VMEM)
     shape = jax.ShapeDtypeStruct
-    return pl.pallas_call(
+    dq, dk, dv, drot, dw = pl.pallas_call(
         kernel,
         out_shape=(
-            shape((ROWS, NOPE + ROPE), BF16),
-            shape((ROWS, NOPE), BF16),
-            shape((ROWS, VAL), BF16),
-            shape((ROWS, ROPE), F32),
+            shape((NOPE + ROPE, ROWS), BF16),
+            shape((NOPE, ROWS), BF16),
+            shape((VAL, ROWS), BF16),
+            shape((ROPE, ROWS), F32),
             shape((8, 128), F32),
         ),
         in_specs=[vmem] * 7,
@@ -320,7 +315,8 @@
             pltpu.SemaphoreType.DMA((COPIES,)),
         ],
         compiler_params=pltpu.CompilerParams(collective_id=0, has_side_effects=True),
-    )(*arrays)
+    )(queries.T, latents, rot_key.T, kv_weight, log_sums.T, outputs.T, out_grad.T)
+    return dq.T, dk.T, dv.T, drot.T, dw
 
 
 def solution(mesh):

time: 67.9 us -> 62.4 us (0.919); the launches traced: 67.4 us -> 61.2 us
  local copies, waits for them, and re-layouts: 9.25 us -> 4.07 us
  Pallas kernels: 57.5 us -> 56.5 us
    pallas_call x4 -> x0, local copies, waits for them, and re-layouts: 4.32 us -> none  [per_device(): pl.pallas_call(kernel, out_shape=(shape((ROWS, NOPE + ROPE), BF16), shape...]
    pallas_call x1, Pallas kernels: 57.5 us -> 56.5 us  [per_device(): pl.pallas_call(kernel, out_shape=(shape((NOPE + ROPE, ROWS), BF16), shape...]
    unnamed x20 -> x13, local copies, waits for them, and re-layouts: 4.93 us -> 4.07 us
where the time goes in v2:
time: 62.4 us; the launch traced here: 61.2 us
  Pallas kernels  56.5 us (91%)
  local copies, waits for them, and re-layouts  4.07 us (7%)
  between operations  0.66 us (1%)
    pallas_call x1, Pallas kernels, per_device(): pl.pallas_call(kernel, out_shape=(shape((NOPE + ROPE, ROWS), BF16), shape...  56.5 us
    unnamed x13, local copies, waits for them, and re-layouts  4.07 us

profile of v2, /device:TPU:6, one launch (start us, length us, event | category | flops | bytes accessed | tf_op | source)
XLA Modules:
  0.0 61.2 jit_solution(6878209177080740064)
XLA Ops:
  0.6 56.5 %shard_map.110 = (bf16[96,128]{1,0:T(8,128)(2,1)}, bf16[64,128]{1,0:T(8,128)(2,1)}, bf16[64,128]{1,0:T(8,128)(2,1)}, f32[32,128]{1,0:T(8,128)}, f32[8,128]{1,0:T(8,128)}) custom-call(bf16[96,128]{1,0:T(8,128)(2,1)} %bitcast.9, bf16[128,512]{1,0:T(8,128)(2,1)} %lat_ref.1, bf16[32,128]{1,0:T(8,128)(2,1)} %bitcast.16, bf16[512,128]{1,0:T(8,128)(2,1)} %w_ref.1, ...), custom_call_target="tpu_custom_call" | custom-call | tf_op jit(solution)/shard_map/pallas_call | solution.py:283
  57.1 0.0 copy-start.2
  57.1 1.4 %copy.17 = bf16[128,96]{0,1:T(8,128)(2,1)} copy(bf16[128,96]{0,1:T(8,128)(2,1)} %bitcast.10) | data formatting | bytes 49152
  58.5 0.0 copy-done.2
  58.5 0.0 copy-start.1
  58.5 0.6 copy.18
  59.1 0.1 copy-done.1
  59.2 0.0 copy-start
  59.2 0.6 copy.19
  59.8 0.1 copy-done
  59.9 0.0 copy-start.3
  59.9 0.6 copy.20
  60.5 0.1 copy-done.3
  60.6 0.6 copy.21
Async XLA Ops:
  57.1 1.4 %copy-start.2 = (bf16[64,128]{1,0:T(8,128)(2,1)S(1)}, bf16[64,128]{1,0:T(8,128)(2,1)}, u32[]{:S(2)}) copy-start(bf16[64,128]{1,0:T(8,128)(2,1)} %get-tuple-element.11) | copy-start | bytes 49156
  58.5 0.7 %copy-start.1 = (bf16[64,128]{1,0:T(8,128)(2,1)S(1)}, bf16[64,128]{1,0:T(8,128)(2,1)}, u32[]{:S(2)}) copy-start(bf16[64,128]{1,0:T(8,128)(2,1)} %get-tuple-element.12) | copy-start | bytes 49156
  59.2 0.7 %copy-start = (f32[32,128]{1,0:T(8,128)S(1)}, f32[32,128]{1,0:T(8,128)}, u32[]{:S(2)}) copy-start(f32[32,128]{1,0:T(8,128)} %get-tuple-element.13) | copy-start | bytes 49156
  59.9 0.7 %copy-start.3 = (f32[8,128]{1,0:T(8,128)S(1)}, f32[8,128]{1,0:T(8,128)}, u32[]{:S(2)}) copy-start(f32[8,128]{1,0:T(8,128)} %get-tuple-element.24) | copy-start | bytes 12292

commit v3 on v2

--- a/solution.py
+++ b/solution.py
@@ -17,6 +17,7 @@
 NY = 4
 NZ = 16
 NTP = 8
+PART = RANK // NTP
 PACK = 176
 SCALE = (NOPE + ROPE) ** -0.5
 LOG2E = 1.4426950408889634
@@ -24,15 +25,17 @@
 Q_FAR = 0
 Q_Y = 3
 KV = 15
-LAT = 18
-DQ_Y = 21
-DQ_Z = 33
-DKV = 36
-DROT = 39
-W_Y = 42
-W_Z = 45
-ROT = 60
-COPIES = 67
+KROT = 18
+LAT = 21
+LAT_TP = 24
+DQ_Y = 31
+DQ_Z = 43
+DKV = 46
+DROT = 49
+W_Y = 52
+W_Z = 55
+ROT = 70
+COPIES = 77
 
 
 def three(x):
@@ -52,17 +55,17 @@
 
 
 def kernel(
-    q_ref, lat_ref, rot_ref, w_ref, lse_ref, o_ref, do_ref,
+    q_hbm, lat_hbm, rot_hbm, w_hbm, lse_hbm, o_hbm, do_hbm,
     dq_ref, dk_ref, dv_ref, drot_ref, dw_ref,
-    qbuf, kvbuf, kt, latt, mbuf, acc, dqp, dqr, dqs, dqz, dkvs, dkvr, rots, rotr, rotx, wsend, wrecv, wzs, wzr,
-    ssem, rsem,
+    q_ref, lat_ref, w_ref, lse_ref, o_ref, do_ref,
+    qbuf, kvm, kvx, krot, kt, latt, mbuf, acc, dqp, dqr, dqs, dqz, dkvs, dkvr, rots, rotr, rotx, wsend, wrecv, wzs, wzr,
+    isem, ssem, rsem,
 ):
     sp = lax.axis_index("sp")
     tp = lax.axis_index("tp")
     z = sp // NY
     y = sp % NY
-    odd = z % 2
-    sign = 1 - 2 * odd
+    sign = 1 - 2 * (z % 2)
 
     def dev(dz, dy):
         return (((z + dz + NZ) % NZ) * NY + (y + dy + NY) % NY, tp)
@@ -76,12 +79,28 @@
             device_id=device, device_id_type=MESH,
         )
 
+    def others(k):
+        return (sp, (tp + k) % NTP)
+
+    loads = [
+        pltpu.make_async_copy(src, dst, isem.at[i])
+        for i, (src, dst) in enumerate((
+            (o_hbm, o_ref), (do_hbm, do_ref), (q_hbm, q_ref), (lse_hbm, lse_ref),
+            (lat_hbm, lat_ref), (w_hbm, w_ref), (rot_hbm, krot.at[0]),
+        ))
+    ]
     barrier = pltpu.get_barrier_semaphore()
-    greet = [dev(d, 0) for d in (1, -1, 2, -2, 4, -4)] + [dev(0, d) for d in (1, -1, 2)]
-    greet += [(sp, (tp + k) % NTP) for k in range(1, NTP)]
+    greet = [dev(d, 0) for d in (4, -4, 1, -1, 2, -2)] + [dev(0, d) for d in (1, -1, 2)]
+    greet += [others(k) for k in range(1, NTP)]
     for device in greet:
         pl.semaphore_signal(barrier, inc=1, device_id=device, device_id_type=MESH)
-
+    for c in loads:
+        c.start()
+    mbuf[...] = jnp.zeros_like(mbuf)
+    acc[...] = jnp.zeros_like(acc)
+
+    for c in loads[0:4]:
+        c.wait()
     delta = jnp.sum(o_ref[...].astype(F32) * do_ref[...].astype(F32), axis=0, keepdims=True)
     lse = lse_ref[...] * (1.0 / SCALE)
     row = lax.broadcasted_iota(jnp.int32, (16, ROWS), 0)
@@ -93,47 +112,47 @@
     qbuf[0, 128:160, :] = q_ref[64:96, :]
     qbuf[0, 160:176, :] = aux.astype(BF16)
 
+    for c in loads[4:7]:
+        c.wait()
+    kvm[0:ROWS, :] = dot(lat_ref[...], w_ref[...]).astype(BF16)
+    latt[0] = jnp.transpose(lat_ref[...].astype(F32)).astype(BF16)
+
     pl.semaphore_wait(barrier, len(greet))
 
+    def rows_of(s):
+        return pl.ds(ROWS * s, ROWS)
+
     q_far = [
-        copy(Q_FAR + 0, qbuf.at[0], qbuf.at[8], dev(-4, 0)),
-        copy(Q_FAR + 1, qbuf.at[0], qbuf.at[4], dev(4, 0)),
-        copy(Q_FAR + 2, qbuf.at[4 + 4 * odd], qbuf.at[12], dev(4 * sign, 0)),
+        copy(Q_FAR + 0, qbuf.at[0], qbuf.at[4], dev(4 * sign, 0)),
+        copy(Q_FAR + 1, qbuf.at[0], qbuf.at[8], dev(-4 * sign, 0)),
+        copy(Q_FAR + 2, qbuf.at[4], qbuf.at[12], dev(4 * sign, 0)),
     ]
-    q_far[0].start()
-    q_far[1].start()
     q_y = [
         [copy(Q_Y + 3 * t + u - 1, qbuf.at[4 * t], qbuf.at[4 * t + u], dev(0, y_off[u])) for u in (1, 2, 3)]
         for t in range(4)
     ]
+    mine = pl.ds(PART * tp, PART)
+    kv = [copy(KV + s - 1, kvm.at[rows_of(0)], kvm.at[rows_of(s)], dev(k_off[s], 0)) for s in (1, 2, 3)]
+    kv += [copy(KROT + s - 1, krot.at[0], krot.at[s], dev(k_off[s], 0)) for s in (1, 2, 3)]
+    lat = [copy(LAT + s - 1, latt.at[0, mine], latt.at[s, mine], dev(k_off[s], 0)) for s in (1, 2, 3)]
+    q_far[0].start()
+    for c in kv:
+        c.start()
+    q_far[1].start()
     for c in q_y[0]:
         c.start()
-
-    joined = dot(lat_ref[...], w_ref[...]).astype(BF16)
-    kvbuf[0:ROWS, 0:128] = joined
+    for c in lat:
+        c.start()
+
+    for c in kv:
+        c.wait_recv()
+    kt[0:64, :] = jnp.transpose(kvm[...].astype(F32))[0:64].astype(BF16)
     lane = lax.broadcasted_iota(jnp.int32, (ROWS, 128), 1)
-    rot_rows = jnp.concatenate([rot_ref[...].astype(F32), jnp.zeros((ROWS - ROPE, ROWS), F32)], axis=0)
     marks = jnp.where((lane >= ROPE) & (lane < ROPE + 6), -1.0, 0.0)
-    kvbuf[0:ROWS, 128:256] = (jnp.transpose(rot_rows) + marks).astype(BF16)
-
-    def rows_of(s):
-        return pl.ds(ROWS * s, ROWS)
-
-    kv = [copy(KV + s - 1, kvbuf.at[rows_of(0)], kvbuf.at[rows_of(s)], dev(k_off[s], 0)) for s in (1, 2, 3)]
-    for c in kv:
-        c.start()
-    latt[0] = jnp.transpose(lat_ref[...].astype(F32)).astype(BF16)
-    lat = [copy(LAT + s - 1, latt.at[0], latt.at[s], dev(k_off[s], 0)) for s in (1, 2, 3)]
-    for c in lat:
-        c.start()
-
-    mbuf[...] = jnp.zeros_like(mbuf)
-    acc[...] = jnp.zeros_like(acc)
-
-    for c in kv:
-        c.wait_recv()
-    kt[0:64, :] = jnp.transpose(kvbuf[:, 0:128].astype(F32))[0:64].astype(BF16)
-    kt[64:96, :] = jnp.transpose(kvbuf[:, 128:256].astype(F32))[0:32].astype(BF16)
+    for s in range(4):
+        rot_rows = jnp.concatenate([krot[s].astype(F32), jnp.zeros((ROWS - ROPE, ROWS), F32)], axis=0)
+        kvx[ROWS * s : ROWS * (s + 1), :] = (jnp.transpose(rot_rows) + marks).astype(BF16)
+        kt[64:96, ROWS * s : ROWS * (s + 1)] = krot[s]
 
     def process(slot):
         mbuf[0:64, 0:128] = qbuf[slot, 0:64, :]
@@ -146,7 +165,7 @@
         total = jnp.zeros((96, ROWS), F32)
         for c in range(2):
             rows = pl.ds(256 * c, 256)
-            both = dot(kvbuf[rows, :], m)
+            both = dot(jnp.concatenate([kvm[rows, :], kvx[rows, :]], axis=1), m)
             probs = jnp.exp2(both[:, 0:128] * (SCALE * LOG2E))
             ds = (probs * both[:, 128:256]).astype(BF16)
             acc[rows, :] += dot_nt(jnp.concatenate([ds, probs.astype(BF16)], axis=1), m)
@@ -171,11 +190,19 @@
         lax.fori_loop(1, 4, step, 0)
 
     q_far[0].wait_recv()
+    q_far[2].start()
+    for c in q_y[1]:
+        c.start()
     q_far[1].wait_recv()
-    q_far[2].start()
-    for t in (1, 2):
-        for c in q_y[t]:
-            c.start()
+    for c in q_y[2]:
+        c.start()
+    for c in lat:
+        c.wait_recv()
+    lat_tp = [
+        copy(LAT_TP + k - 1, latt.at[pl.ds(1, 3), mine], latt.at[pl.ds(1, 3), mine], others(k)) for k in range(1, NTP)
+    ]
+    for c in lat_tp:
+        c.start()
     steps(0, True)
     process(4)
     process(8)
@@ -187,7 +214,7 @@
     steps(3, True)
 
     lane_scale = jnp.where(lane < NOPE, SCALE, 1.0)
-    for c in lat:
+    for c in lat_tp:
         c.wait_recv()
     wpart = jnp.zeros((RANK, 128), F32)
     dkv = []
@@ -212,24 +239,20 @@
         w_y.append(copy(W_Y + u - 1, wsend.at[(y + y_off[u] + NY) % NY], wrecv.at[u - 1], dev(0, y_off[u])))
         w_y[-1].start()
 
-    def dq_sum(t):
+    dq_z = []
+    for t, dz in ((1, -4 * sign), (2, 4 * sign), (3, 8), (0, 0)):
         for u in (1, 2, 3):
             dq_y(t, u, dev(0, 1)).wait_recv()
         dqs[t] = dqp[4 * t] + dqr[3 * t] + dqr[3 * t + 1] + dqr[3 * t + 2]
-
-    for t in (3, 1, 2, 0):
-        dq_sum(t)
-        if t == 3:
-            dq_relay = copy(DQ_Z, dqs.at[3], dqz.at[0], dev(4 * sign, 0))
-            dq_relay.start()
-    dq_plain = copy(DQ_Z + 1, dqs.at[1 + odd], dqz.at[1], dev(-4 * sign, 0))
-    dq_plain.start()
+        if t:
+            dq_z.append(copy(DQ_Z + t - 1, dqs.at[t], dqz.at[t - 1], dev(dz, 0)))
+            dq_z[-1].start()
 
     for c in w_y:
         c.wait_recv()
     wzs[...] = wsend[y] + wrecv[0] + wrecv[1] + wrecv[2]
     w_z = []
-    for d in range(1, NZ):
+    for d in (8, 7, 9, 6, 10, 5, 11, 4, 12, 3, 13, 2, 14, 1, 15):
         w_z.append(copy(W_Z + d - 1, wzs.at[(z + d) % NZ], wzr.at[d - 1], dev(d, 0)))
         w_z[-1].start()
 
@@ -239,19 +262,14 @@
     rotx[tp] = rots[0] + rotr[0] + rotr[1] + rotr[2]
     rot = []
     for k in range(1, NTP):
-        rot.append(copy(ROT + k - 1, rotx.at[tp], rotx.at[tp], (sp, (tp + k) % NTP)))
+        rot.append(copy(ROT + k - 1, rotx.at[tp], rotx.at[tp], others(k)))
         rot[-1].start()
     own = jnp.transpose(own).astype(BF16)
     dk_ref[...] = own[0:NOPE]
     dv_ref[...] = own[NOPE:128]
 
-    dq_relay.wait_recv()
-    dqs[2 - odd] = dqs[2 - odd] + dqz[0]
-    dq_last = copy(DQ_Z + 2, dqs.at[2 - odd], dqz.at[2], dev(4 * sign, 0))
-    dq_last.start()
-
-    for k in range(1, NTP):
-        rot[k - 1].wait_recv()
+    for c in rot:
+        c.wait_recv()
     total = rotx[0]
     for k in range(1, NTP):
         total = total + rotx[k]
@@ -264,11 +282,11 @@
         wsum = wsum + wzr[d - 1]
     dw_ref[...] = wsum
 
-    dq_plain.wait_recv()
-    dq_last.wait_recv()
-    dq_ref[...] = ((dqs[0] + dqz[1] + dqz[2]) * SCALE).astype(BF16)
-
-    for c in q_far + kv + lat + dkv + w_y + w_z + rot + [dq_relay, dq_plain, dq_last]:
+    for c in dq_z:
+        c.wait_recv()
+    dq_ref[...] = ((dqs[0] + dqz[0] + dqz[1] + dqz[2]) * SCALE).astype(BF16)
+
+    for c in q_far + kv + lat + lat_tp + dkv + w_y + w_z + rot + dq_z:
         c.wait_send()
     for t in range(4):
         for c in q_y[t]:
@@ -277,23 +295,37 @@
             dq_y(t, u, dev(0, 1)).wait_send()
 
 
+def hand_over(*refs):
+    for src, dst in zip(refs[:5], refs[5:]):
+        dst[...] = src[...]
+
+
 def per_device(queries, latents, rot_key, kv_weight, log_sums, outputs, out_grad):
     vmem = pl.BlockSpec(memory_space=pltpu.VMEM)
     shape = jax.ShapeDtypeStruct
-    dq, dk, dv, drot, dw = pl.pallas_call(
+    results = (
+        shape((NOPE + ROPE, ROWS), BF16),
+        shape((NOPE, ROWS), BF16),
+        shape((VAL, ROWS), BF16),
+        shape((ROPE, ROWS), F32),
+        shape((8, 128), F32),
+    )
+    made = pl.pallas_call(
         kernel,
-        out_shape=(
-            shape((NOPE + ROPE, ROWS), BF16),
-            shape((NOPE, ROWS), BF16),
-            shape((VAL, ROWS), BF16),
-            shape((ROPE, ROWS), F32),
-            shape((8, 128), F32),
-        ),
-        in_specs=[vmem] * 7,
+        out_shape=results,
+        in_specs=[pl.BlockSpec(memory_space=pl.ANY)] * 7,
         out_specs=(vmem,) * 5,
         scratch_shapes=[
+            pltpu.VMEM((NOPE + ROPE, ROWS), BF16),
+            pltpu.VMEM((ROWS, RANK), BF16),
+            pltpu.VMEM((RANK, 128), BF16),
+            pltpu.VMEM((1, ROWS), F32),
+            pltpu.VMEM((VAL, ROWS), BF16),
+            pltpu.VMEM((VAL, ROWS), BF16),
             pltpu.VMEM((16, PACK, ROWS), BF16),
-            pltpu.VMEM((4 * ROWS, 256), BF16),
+            pltpu.VMEM((4 * ROWS, 128), BF16),
+            pltpu.VMEM((4 * ROWS, 128), BF16),
+            pltpu.VMEM((4, ROPE, ROWS), BF16),
             pltpu.VMEM((96, 4 * ROWS), BF16),
             pltpu.VMEM((4, RANK, ROWS), BF16),
             pltpu.VMEM((256, 256), BF16),
@@ -311,11 +343,15 @@
             pltpu.VMEM((3, NZ, 8, 128), F32),
             pltpu.VMEM((NZ, 8, 128), F32),
             pltpu.VMEM((NZ - 1, 8, 128), F32),
+            pltpu.SemaphoreType.DMA((7,)),
             pltpu.SemaphoreType.DMA((COPIES,)),
             pltpu.SemaphoreType.DMA((COPIES,)),
         ],
         compiler_params=pltpu.CompilerParams(collective_id=0, has_side_effects=True),
     )(queries.T, latents, rot_key.T, kv_weight, log_sums.T, outputs.T, out_grad.T)
+    dq, dk, dv, drot, dw = pl.pallas_call(
+        hand_over, out_shape=results, in_specs=[vmem] * 5, out_specs=(vmem,) * 5
+    )(*made)
     return dq.T, dk.T, dv.T, drot.T, dw
 
 

time: 62.4 us -> 54.9 us (0.88); the launches traced: 61.2 us -> 54.3 us
  local copies, waits for them, and re-layouts: 4.07 us -> 0 us
  Pallas kernels: 56.5 us -> 53.7 us
    unnamed x13 -> x0, local copies, waits for them, and re-layouts: 4.07 us -> none
    pallas_call x1 -> x2, Pallas kernels: 56.5 us -> 53.7 us  [the longest x1 52.3 us: per_device(): pl.pallas_call(kernel, out_shape=results, in_specs=[pl.BlockSpec(memory_s...]
where the time goes in v3:
time: 54.9 us; the launch traced here: 54.3 us
  Pallas kernels  53.7 us (98%)
  between operations  0.64 us (1%)
    pallas_call x1, Pallas kernels, per_device(): pl.pallas_call(kernel, out_shape=results, in_specs=[pl.BlockSpec(memory_s...  52.3 us
    pallas_call x1, Pallas kernels, per_device(): pl.pallas_call(hand_over, out_shape=results, in_specs=[vmem] * 5, out_spe...  1.41 us

profile of v3, /device:TPU:6, one launch (start us, length us, event | category | flops | bytes accessed | tf_op | source)
XLA Modules:
  0.0 54.3 jit_solution(17715157002168272423)
XLA Ops:
  0.6 52.3 %shard_map.110 = (bf16[96,128]{1,0:T(8,128)(2,1)}, bf16[64,128]{1,0:T(8,128)(2,1)}, bf16[64,128]{1,0:T(8,128)(2,1)}, f32[32,128]{1,0:T(8,128)}, f32[8,128]{1,0:T(8,128)}) custom-call(bf16[96,128]{1,0:T(8,128)(2,1)} %bitcast.9, bf16[128,512]{1,0:T(8,128)(2,1)} %lat_hbm.1, bf16[32,128]{1,0:T(8,128)(2,1)} %bitcast.12, bf16[512,128]{1,0:T(8,128)(2,1)} %w_hbm.1, ...), custom_call_target="tpu_custom_call" | custom-call | tf_op jit(solution)/shard_map/pallas_call | solution.py:313
  52.9 1.4 %shard_map.111 = (bf16[96,128]{1,0:T(8,128)(2,1)}, bf16[64,128]{1,0:T(8,128)(2,1)}, bf16[64,128]{1,0:T(8,128)(2,1)}, f32[32,128]{1,0:T(8,128)}, f32[8,128]{1,0:T(8,128)}) custom-call(bf16[96,128]{1,0:T(8,128)(2,1)} %get-tuple-element.15.refs_0_, bf16[64,128]{1,0:T(8,128)(2,1)} %get-tuple-element.16.refs_1_, bf16[64,128]{1,0:T(8,128)(2,1)} %get-tuple-element.17.refs_2_, ...), custom_call_target="tpu_custom_call" | custom-call | tf_op jit(solution)/shard_map/pallas_call | solution.py:352

commit v4 on v3

--- a/solution.py
+++ b/solution.py
@@ -58,7 +58,7 @@
     q_hbm, lat_hbm, rot_hbm, w_hbm, lse_hbm, o_hbm, do_hbm,
     dq_ref, dk_ref, dv_ref, drot_ref, dw_ref,
     q_ref, lat_ref, w_ref, lse_ref, o_ref, do_ref,
-    qbuf, kvm, kvx, krot, kt, latt, mbuf, acc, dqp, dqr, dqs, dqz, dkvs, dkvr, rots, rotr, rotx, wsend, wrecv, wzs, wzr,
+    qbuf, kvm, kvx, krot, kt, latt, mbuf, acc, dqp, dqr, dqs, dqz, dkvs, dkvr, halves, rots, rotr, rotx, wsend, wrecv, wzs, wzr,
     isem, ssem, rsem,
 ):
     sp = lax.axis_index("sp")
@@ -178,15 +178,13 @@
     def back(u):
         return dev(0, jnp.where(u == 1, -1, jnp.where(u == 2, 1, 2)))
 
-    def steps(t, first):
+    def steps(t):
         def step(u, carry):
             copy(Q_Y + 3 * t + u - 1, qbuf.at[4 * t], qbuf.at[4 * t + u], dev(0, 1)).wait_recv()
             process(4 * t + u)
             dq_y(t, u, back(u)).start()
             return carry
 
-        if first:
-            process(4 * t)
         lax.fori_loop(1, 4, step, 0)
 
     q_far[0].wait_recv()
@@ -203,35 +201,53 @@
     ]
     for c in lat_tp:
         c.start()
-    steps(0, True)
+    process(0)
+    steps(0)
     process(4)
     process(8)
+    steps(1)
+    steps(2)
     q_far[2].wait_recv()
     for c in q_y[3]:
         c.start()
-    steps(1, False)
-    steps(2, False)
-    steps(3, True)
+    process(12)
+
+    def dq_sum(t):
+        for u in (1, 2, 3):
+            dq_y(t, u, dev(0, 1)).wait_recv()
+        return dqp[4 * t] + dqr[3 * t] + dqr[3 * t + 1] + dqr[3 * t + 2]
+
+    dq_z = []
+
+    def dq_send(t, dz):
+        dqs[t - 1] = dq_sum(t).astype(BF16)
+        dq_z.append(copy(DQ_Z + t - 1, dqs.at[t - 1], dqz.at[t - 1], dev(dz, 0)))
+        dq_z[-1].start()
+
+    dq_send(1, -4 * sign)
+    dq_send(2, 4 * sign)
+    steps(3)
 
     lane_scale = jnp.where(lane < NOPE, SCALE, 1.0)
-    for c in lat_tp:
-        c.wait_recv()
-    wpart = jnp.zeros((RANK, 128), F32)
     dkv = []
     for s in (1, 2, 3, 0):
         main = acc[ROWS * s : ROWS * (s + 1), 0:128] * lane_scale
-        dkvs[s] = main
+        hi = main.astype(BF16)
+        halves[ROWS * s : ROWS * (s + 1), 0:128] = hi
+        halves[ROWS * s : ROWS * (s + 1), 128:256] = (main - hi.astype(F32)).astype(BF16)
         rots[s] = jnp.transpose(acc[ROWS * s : ROWS * (s + 1), 128:256])[0:ROPE] * SCALE
         if s:
+            dkvs[s - 1] = hi
             owner = dev(-k_off[s], 0)
-            dkv.append(copy(DKV + s - 1, dkvs.at[s], dkvr.at[s - 1], owner))
+            dkv.append(copy(DKV + s - 1, dkvs.at[s - 1], dkvr.at[s - 1], owner))
             dkv.append(copy(DROT + s - 1, rots.at[s], rotr.at[s - 1], owner))
             dkv[-2].start()
             dkv[-1].start()
-        hi = main.astype(BF16)
-        low = (main - hi.astype(F32)).astype(BF16)
-        wpart = wpart + dot(latt[s], hi) + dot(latt[s], low)
-    wpart = wpart.reshape(NZ, NY, 8, 128)
+    for c in lat_tp:
+        c.wait_recv()
+    lat_all = jnp.concatenate([latt[0], latt[1], latt[2], latt[3]], axis=1)
+    wpart = dot(lat_all, halves[...])
+    wpart = (wpart[:, 0:128] + wpart[:, 128:256]).reshape(NZ, NY, 8, 128)
     for v in range(NY):
         wsend[v] = wpart[:, v]
     w_y = []
@@ -239,14 +255,7 @@
         w_y.append(copy(W_Y + u - 1, wsend.at[(y + y_off[u] + NY) % NY], wrecv.at[u - 1], dev(0, y_off[u])))
         w_y[-1].start()
 
-    dq_z = []
-    for t, dz in ((1, -4 * sign), (2, 4 * sign), (3, 8), (0, 0)):
-        for u in (1, 2, 3):
-            dq_y(t, u, dev(0, 1)).wait_recv()
-        dqs[t] = dqp[4 * t] + dqr[3 * t] + dqr[3 * t + 1] + dqr[3 * t + 2]
-        if t:
-            dq_z.append(copy(DQ_Z + t - 1, dqs.at[t], dqz.at[t - 1], dev(dz, 0)))
-            dq_z[-1].start()
+    dq_send(3, 8)
 
     for c in w_y:
         c.wait_recv()
@@ -258,7 +267,9 @@
 
     for c in dkv:
         c.wait_recv()
-    own = dkvs[0] + dkvr[0] + dkvr[1] + dkvr[2]
+    own = acc[0:ROWS, 0:128] * lane_scale
+    for s in range(3):
+        own = own + dkvr[s].astype(F32)
     rotx[tp] = rots[0] + rotr[0] + rotr[1] + rotr[2]
     rot = []
     for k in range(1, NTP):
@@ -282,9 +293,12 @@
         wsum = wsum + wzr[d - 1]
     dw_ref[...] = wsum
 
+    total = dq_sum(0)
     for c in dq_z:
         c.wait_recv()
-    dq_ref[...] = ((dqs[0] + dqz[0] + dqz[1] + dqz[2]) * SCALE).astype(BF16)
+    for t in range(3):
+        total = total + dqz[t].astype(F32)
+    dq_ref[...] = (total * SCALE).astype(BF16)
 
     for c in q_far + kv + lat + lat_tp + dkv + w_y + w_z + rot + dq_z:
         c.wait_send()
@@ -332,10 +346,11 @@
             pltpu.VMEM((4 * ROWS, 256), F32),
             pltpu.VMEM((16, 96, ROWS), F32),
             pltpu.VMEM((12, 96, ROWS), F32),
-            pltpu.VMEM((4, 96, ROWS), F32),
-            pltpu.VMEM((3, 96, ROWS), F32),
-            pltpu.VMEM((4, ROWS, 128), F32),
-            pltpu.VMEM((3, ROWS, 128), F32),
+            pltpu.VMEM((3, 96, ROWS), BF16),
+            pltpu.VMEM((3, 96, ROWS), BF16),
+            pltpu.VMEM((3, ROWS, 128), BF16),
+            pltpu.VMEM((3, ROWS, 128), BF16),
+            pltpu.VMEM((4 * ROWS, 256), BF16),
             pltpu.VMEM((4, ROPE, ROWS), F32),
             pltpu.VMEM((3, ROPE, ROWS), F32),
             pltpu.VMEM((NTP, ROPE, ROWS), F32),

time: 54.9 us -> 52 us (0.947)
  Pallas kernels: 53.7 us -> 50.8 us
    pallas_call x1, Pallas kernels: 52.3 us -> 49.4 us  [per_device(): pl.pallas_call(kernel, out_shape=results, in_specs=[pl.BlockSpec(memory_s...]
where the time goes in v4:
time: 52 us; the launch traced here: 51.5 us
  Pallas kernels  50.8 us (98%)
  between operations  0.64 us (1%)
    pallas_call x1, Pallas kernels, per_device(): pl.pallas_call(kernel, out_shape=results, in_specs=[pl.BlockSpec(memory_s...  49.4 us
    pallas_call x1, Pallas kernels, per_device(): pl.pallas_call(hand_over, out_shape=results, in_specs=[vmem] * 5, out_spe...  1.41 us

profile of v4, /device:TPU:6, one launch (start us, length us, event | category | flops | bytes accessed | tf_op | source)
XLA Modules:
  0.0 51.5 jit_solution(14518584184763652085)
XLA Ops:
  0.6 49.4 %shard_map.110 = (bf16[96,128]{1,0:T(8,128)(2,1)}, bf16[64,128]{1,0:T(8,128)(2,1)}, bf16[64,128]{1,0:T(8,128)(2,1)}, f32[32,128]{1,0:T(8,128)}, f32[8,128]{1,0:T(8,128)}) custom-call(bf16[96,128]{1,0:T(8,128)(2,1)} %bitcast.9, bf16[128,512]{1,0:T(8,128)(2,1)} %lat_hbm.1, bf16[32,128]{1,0:T(8,128)(2,1)} %bitcast.12, bf16[512,128]{1,0:T(8,128)(2,1)} %w_hbm.1, ...), custom_call_target="tpu_custom_call" | custom-call | tf_op jit(solution)/shard_map/pallas_call | solution.py:327
  50.1 1.4 %shard_map.111 = (bf16[96,128]{1,0:T(8,128)(2,1)}, bf16[64,128]{1,0:T(8,128)(2,1)}, bf16[64,128]{1,0:T(8,128)(2,1)}, f32[32,128]{1,0:T(8,128)}, f32[8,128]{1,0:T(8,128)}) custom-call(bf16[96,128]{1,0:T(8,128)(2,1)} %get-tuple-element.15.refs_0_, bf16[64,128]{1,0:T(8,128)(2,1)} %get-tuple-element.16.refs_1_, bf16[64,128]{1,0:T(8,128)(2,1)} %get-tuple-element.17.refs_2_, ...), custom_call_target="tpu_custom_call" | custom-call | tf_op jit(solution)/shard_map/pallas_call | solution.py:367

commit v5 on v3

v5 whole, which is shorter than its diff:
```python
import jax
import jax.numpy as jnp
from jax import lax
from jax.experimental import pallas as pl
from jax.experimental.pallas import tpu as pltpu
from jax.sharding import PartitionSpec as P

MESH = pl.DeviceIdType.MESH
F32 = jnp.float32
BF16 = jnp.bfloat16

NOPE = 64
ROPE = 32
VAL = 64
RANK = 512
ROWS = 128
NY = 4
NZ = 16
NTP = 8
PART = RANK // NTP
PACK = 176
SCALE = (NOPE + ROPE) ** -0.5
LOG2E = 1.4426950408889634

K_FAR = 0
K_ROT = 3
LAT = 6
LAT_TP = 9
Q_N = 23
Q_Y = 26
DQ_Y = 38
DQ_N = 50
DKV = 53
DROT = 56
W_Y = 59
W_Z = 62
ROT = 77
COPIES = 84


def three(x):
    hi = x.astype(BF16)
    rest = x - hi.astype(F32)
    mid = rest.astype(BF16)
    low = (rest - mid.astype(F32)).astype(BF16)
    return [hi.astype(F32), mid.astype(F32), low.astype(F32)]


def dot(a, b):
    return jnp.dot(a, b, preferred_element_type=F32)


def dot_nt(a, b):
    return lax.dot_general(a, b, (((1,), (1,)), ((), ())), preferred_element_type=F32)


def kernel(
    q_hbm, lat_hbm, rot_hbm, w_hbm, lse_hbm, o_hbm, do_hbm,
    dq_ref, dk_ref, dv_ref, drot_ref, dw_ref,
    q_ref, lat_ref, w_ref, lse_ref, o_ref, do_ref,
    qbuf, kvm, kvx, krot, kt, latt, mall, acc, dqp, dqb, dqr, dqs, dqz, dkvs, dkvr, halves, rots, rotr, rotx,
    wsend, wrecv, wzs, wzr,
    isem, ssem, rsem,
):
    sp = lax.axis_index("sp")
    tp = lax.axis_index("tp")
    z = sp // NY
    y = sp % NY
    sign = 1 - 2 * (z % 2)

    def dev(dz, dy):
        return (((z + dz + NZ) % NZ) * NY + (y + dy + NY) % NY, tp)

    y_off = (0, 1, -1, 2)
    n_off = (0, 1, -1, 2 * sign)
    f_off = (0, 4 * sign, -4 * sign, 8)

    def copy(number, src, dst, device):
        return pltpu.make_async_remote_copy(
            src_ref=src, dst_ref=dst, send_sem=ssem.at[number], recv_sem=rsem.at[number],
            device_id=device, device_id_type=MESH,
        )

    def others(k):
        return (sp, (tp + k) % NTP)

    def rows_of(t):
        return pl.ds(ROWS * t, ROWS)

    loads = [
        pltpu.make_async_copy(src, dst, isem.at[i])
        for i, (src, dst) in enumerate((
            (lat_hbm, lat_ref), (w_hbm, w_ref), (rot_hbm, krot.at[0]),
            (o_hbm, o_ref), (do_hbm, do_ref), (q_hbm, q_ref), (lse_hbm, lse_ref),
        ))
    ]
    barrier = pltpu.get_barrier_semaphore()
    greet = [dev(d, 0) for d in (4, -4, 1, -1, 2, -2)] + [dev(0, d) for d in (1, -1, 2)]
    greet += [others(k) for k in range(1, NTP)]
    for device in greet:
        pl.semaphore_signal(barrier, inc=1, device_id=device, device_id_type=MESH)
    for c in loads:
        c.start()
    mall[...] = jnp.zeros_like(mall)
    acc[...] = jnp.zeros_like(acc)

    for c in loads[0:3]:
        c.wait()
    kvm[0:ROWS, :] = dot(lat_ref[...], w_ref[...]).astype(BF16)
    latt[0] = jnp.transpose(lat_ref[...].astype(F32)).astype(BF16)

    for c in loads[3:7]:
        c.wait()
    delta = jnp.sum(o_ref[...].astype(F32) * do_ref[...].astype(F32), axis=0, keepdims=True)
    lse = lse_ref[...] * (1.0 / SCALE)
    row = lax.broadcasted_iota(jnp.int32, (16, ROWS), 0)
    aux = jnp.zeros((16, ROWS), F32)
    for i, piece in enumerate(three(lse) + three(delta)):
        aux = jnp.where(row == i, jnp.broadcast_to(piece, (16, ROWS)), aux)
    qbuf[0, 0:64, :] = q_ref[0:64, :]
    qbuf[0, 64:128, :] = do_ref[...]
    qbuf[0, 128:160, :] = q_ref[64:96, :]
    qbuf[0, 160:176, :] = aux.astype(BF16)

    pl.semaphore_wait(barrier, len(greet))

    mine = pl.ds(PART * tp, PART)
    far = [
        [
            copy(K_FAR + t - 1, kvm.at[rows_of(a)], kvm.at[rows_of(t)], device),
            copy(K_ROT + t - 1, krot.at[a], krot.at[t], device),
            copy(LAT + t - 1, latt.at[a, mine], latt.at[t, mine], device),
        ]
        for t, a, device in ((1, 0, dev(4 * sign, 0)), (2, 0, dev(-4 * sign, 0)), (3, 1, dev(4 * sign, 0)))
    ]
    q_n = [copy(Q_N + s - 1, qbuf.at[0], qbuf.at[4 * s], dev(n_off[s], 0)) for s in (1, 2, 3)]
    q_y = [
        [copy(Q_Y + 3 * s + u - 1, qbuf.at[4 * s], qbuf.at[4 * s + u], dev(0, y_off[u])) for u in (1, 2, 3)]
        for s in range(4)
    ]
    for c in far[0] + q_n + far[1] + q_y[0]:
        c.start()
    for s in (1, 2, 3):
        q_n[s - 1].wait_recv()
        for c in q_y[s]:
            c.start()

    lane = lax.broadcasted_iota(jnp.int32, (ROWS, 128), 1)
    marks = jnp.where((lane >= ROPE) & (lane < ROPE + 6), -1.0, 0.0)

    def prepare(t):
        here = slice(ROWS * t, ROWS * (t + 1))
        kt[0:64, here] = jnp.transpose(kvm[here, :].astype(F32))[0:64].astype(BF16)
        kt[64:96, here] = krot[t]
        rot_rows = jnp.concatenate([krot[t].astype(F32), jnp.zeros((ROWS - ROPE, ROWS), F32)], axis=0)
        kvx[here, :] = (jnp.transpose(rot_rows) + marks).astype(BF16)

    prepare(0)
    for i in range(3):
        far[0][i].wait_recv()
        far[2][i].start()
    for c in far[1]:
        c.wait_recv()
    share = [
        copy(LAT_TP + k - 1, latt.at[pl.ds(1, 2), mine], latt.at[pl.ds(1, 2), mine], others(k)) for k in range(1, NTP)
    ]
    for c in share:
        c.start()
    prepare(1)
    prepare(2)

    def tile(s, first, count):
        m = mall[s]
        deltas = []
        for t in range(first, first + count):
            here = slice(ROWS * t, ROWS * (t + 1))
            both = dot(jnp.concatenate([kvm[here, :], kvx[here, :]], axis=1), m)
            ds, mixed = [], []
            for u in range(4):
                probs = jnp.exp2(both[:, 256 * u : 256 * u + 128] * (SCALE * LOG2E))
                ds.append((probs * both[:, 256 * u + 128 : 256 * u + 256]).astype(BF16))
                mixed += [ds[-1], probs.astype(BF16)]
            acc[here, :] += dot_nt(jnp.concatenate(mixed, axis=1), m)
            deltas.append(jnp.concatenate(ds, axis=1))
        deltas = deltas[0] if count == 1 else jnp.concatenate(deltas, axis=0)
        return dot(kt[:, ROWS * first : ROWS * (first + count)], deltas)

    def early(s, carry):
        for u in range(4):
            if u:
                copy(Q_Y + 3 * s + u - 1, qbuf.at[4 * s], qbuf.at[4 * s + u], dev(0, 1)).wait_recv()
            slot, at = 4 * s + u, 256 * u
            mall[s, 0:64, at : at + 128] = qbuf[slot, 0:64, :]
            mall[s, 64:128, at + 128 : at + 256] = qbuf[slot, 64:128, :]
            mall[s, 128:160, at : at + 128] = qbuf[slot, 128:160, :]
            extra = qbuf[slot, 160:176, :].astype(F32)
            mall[s, 160:176, at : at + 128] = jnp.where(row < 3, extra, 0.0).astype(BF16)
            mall[s, 160:176, at + 128 : at + 256] = jnp.where(row >= 3, extra, 0.0).astype(BF16)
        dqp[s] = tile(s, 0, 3)
        return carry

    lax.fori_loop(0, 4, early, 0)

    lane_scale = jnp.where(lane < NOPE, SCALE, 1.0)
    dkv, drot = [], []

    def finish(t):
        here = slice(ROWS * t, ROWS * (t + 1))
        main = acc[here, 0:128] * lane_scale
        hi = main.astype(BF16)
        rots[t] = jnp.transpose(acc[here, 128:256])[0:ROPE] * SCALE
        if t:
            dkvs[t - 1] = hi
            owner = dev(-f_off[t], 0)
            drot.append(copy(DROT + t - 1, rots.at[t], rotr.at[t - 1], owner))
            drot[-1].start()
            dkv.append(copy(DKV + t - 1, dkvs.at[t - 1], dkvr.at[t - 1], owner))
            dkv[-1].start()
        halves[here, 0:128] = hi
        halves[here, 128:256] = (main - hi.astype(F32)).astype(BF16)

    for t in (1, 2, 0):
        finish(t)
    for c in share:
        c.wait_recv()
    wpart = dot(jnp.concatenate([latt[0], latt[1], latt[2]], axis=1), halves[0 : 3 * ROWS, :])
    wpart = wpart[:, 0:128] + wpart[:, 128:256]

    for c in far[2]:
        c.wait_recv()
    share_last = [copy(LAT_TP + 6 + k, latt.at[3, mine], latt.at[3, mine], others(k)) for k in range(1, NTP)]
    for c in share_last:
        c.start()
    prepare(3)

    def late(s, carry):
        total = dqp[s] + tile(s, 3, 1)
        dqp[s] = total
        for u in (1, 2, 3):
            dqb[4 * s + u] = total[:, 128 * u : 128 * u + 128].astype(BF16)
        return carry

    lax.fori_loop(0, 4, late, 0)

    finish(3)
    for c in share_last:
        c.wait_recv()
    more = dot(latt[3], halves[3 * ROWS : 4 * ROWS, :])
    wpart = (wpart + more[:, 0:128] + more[:, 128:256]).reshape(NZ, NY, 8, 128)
    for v in range(NY):
        wsend[v] = wpart[:, v]
    w_y = []
    for u in (1, 2, 3):
        w_y.append(copy(W_Y + u - 1, wsend.at[(y + y_off[u] + NY) % NY], wrecv.at[u - 1], dev(0, y_off[u])))
        w_y[-1].start()

    dq_y = [
        [copy(DQ_Y + 3 * s + u - 1, dqb.at[4 * s + u], dqr.at[3 * s + u - 1], dev(0, -y_off[u])) for u in (1, 2, 3)]
        for s in range(4)
    ]
    for s in (3, 1, 2, 0):
        for c in dq_y[s]:
            c.start()

    def dq_sum(s):
        total = dqp[s, :, 0:128]
        for u in (1, 2, 3):
            dq_y[s][u - 1].wait_recv()
            total = total + dqr[3 * s + u - 1].astype(F32)
        return total

    for c in w_y:
        c.wait_recv()
    wzs[...] = wsend[y] + wrecv[0] + wrecv[1] + wrecv[2]
    w_z = []
    for d in (8, 7, 9, 6, 10, 5, 11, 4, 12, 3, 13, 2, 14, 1, 15):
        w_z.append(copy(W_Z + d - 1, wzs.at[(z + d) % NZ], wzr.at[d - 1], dev(d, 0)))
        w_z[-1].start()

    dq_n = []
    for s in (3, 1, 2):
        dqs[s - 1] = dq_sum(s)
        dq_n.append(copy(DQ_N + s - 1, dqs.at[s - 1], dqz.at[s - 1], dev(-n_off[s], 0)))
        dq_n[-1].start()

    for c in drot:
        c.wait_recv()
    rotx[tp] = rots[0] + rotr[0] + rotr[1] + rotr[2]
    rot = []
    for k in range(1, NTP):
        rot.append(copy(ROT + k - 1, rotx.at[tp], rotx.at[tp], others(k)))
        rot[-1].start()

    for c in dkv:
        c.wait_recv()
    own = acc[0:ROWS, 0:128] * lane_scale
    for t in range(3):
        own = own + dkvr[t].astype(F32)
    own = jnp.transpose(own).astype(BF16)
    dk_ref[...] = own[0:NOPE]
    dv_ref[...] = own[NOPE:128]

    total = dq_sum(0)
    for c in dq_n:
        c.wait_recv()
    dq_ref[...] = ((total + dqz[0] + dqz[1] + dqz[2]) * SCALE).astype(BF16)

    for c in rot:
        c.wait_recv()
    total = rotx[0]
    for k in range(1, NTP):
        total = total + rotx[k]
    drot_ref[...] = total

    for c in w_z:
        c.wait_recv()
    wsum = wzs[z]
    for d in range(1, NZ):
        wsum = wsum + wzr[d - 1]
    dw_ref[...] = wsum

    for c in q_n + share + share_last + dkv + drot + w_y + w_z + rot + dq_n:
        c.wait_send()
    for group in far + q_y + dq_y:
        for c in group:
            c.wait_send()


def hand_over(*refs):
    for src, dst in zip(refs[:5], refs[5:]):
        dst[...] = src[...]


def per_device(queries, latents, rot_key, kv_weight, log_sums, outputs, out_grad):
    vmem = pl.BlockSpec(memory_space=pltpu.VMEM)
    shape = jax.ShapeDtypeStruct
    results = (
        shape((NOPE + ROPE, ROWS), BF16),
        shape((NOPE, ROWS), BF16),
        shape((VAL, ROWS), BF16),
        shape((ROPE, ROWS), F32),
        shape((8, 128), F32),
    )
    made = pl.pallas_call(
        kernel,
        out_shape=results,
        in_specs=[pl.BlockSpec(memory_space=pl.ANY)] * 7,
        out_specs=(vmem,) * 5,
        scratch_shapes=[
            pltpu.VMEM((NOPE + ROPE, ROWS), BF16),
            pltpu.VMEM((ROWS, RANK), BF16),
            pltpu.VMEM((RANK, 128), BF16),
            pltpu.VMEM((1, ROWS), F32),
            pltpu.VMEM((VAL, ROWS), BF16),
            pltpu.VMEM((VAL, ROWS), BF16),
            pltpu.VMEM((16, PACK, ROWS), BF16),
            pltpu.VMEM((4 * ROWS, 128), BF16),
            pltpu.VMEM((4 * ROWS, 128), BF16),
            pltpu.VMEM((4, ROPE, ROWS), BF16),
            pltpu.VMEM((96, 4 * ROWS), BF16),
            pltpu.VMEM((4, RANK, ROWS), BF16),
            pltpu.VMEM((4, 256, 1024), BF16),
            pltpu.VMEM((4 * ROWS, 256), F32),
            pltpu.VMEM((4, 96, 4 * ROWS), F32),
            pltpu.VMEM((16, 96, ROWS), BF16),
            pltpu.VMEM((12, 96, ROWS), BF16),
            pltpu.VMEM((3, 96, ROWS), F32),
            pltpu.VMEM((3, 96, ROWS), F32),
            pltpu.VMEM((3, ROWS, 128), BF16),
            pltpu.VMEM((3, ROWS, 128), BF16),
            pltpu.VMEM((4 * ROWS, 256), BF16),
            pltpu.VMEM((4, ROPE, ROWS), F32),
            pltpu.VMEM((3, ROPE, ROWS), F32),
            pltpu.VMEM((NTP, ROPE, ROWS), F32),
            pltpu.VMEM((NY, NZ, 8, 128), F32),
            pltpu.VMEM((3, NZ, 8, 128), F32),
            pltpu.VMEM((NZ, 8, 128), F32),
            pltpu.VMEM((NZ - 1, 8, 128), F32),
            pltpu.SemaphoreType.DMA((7,)),
            pltpu.SemaphoreType.DMA((COPIES,)),
            pltpu.SemaphoreType.DMA((COPIES,)),
        ],
        compiler_params=pltpu.CompilerParams(collective_id=0, has_side_effects=True),
    )(queries.T, latents, rot_key.T, kv_weight, log_sums.T, outputs.T, out_grad.T)
    dq, dk, dv, drot, dw = pl.pallas_call(
        hand_over, out_shape=results, in_specs=[vmem] * 5, out_specs=(vmem,) * 5
    )(*made)
    return dq.T, dk.T, dv.T, drot.T, dw


def solution(mesh):
    placed = (
        P("sp", "tp"),
        P("sp", None),
        P("sp", None),
        P(None, "tp"),
        P("sp", "tp"),
        P("sp", "tp"),
        P("sp", "tp"),
    )
    return jax.shard_map(
        per_device,
        mesh=mesh,
        in_specs=placed,
        out_specs=(P("sp", "tp"), P("sp", "tp"), P("sp", "tp"), P("sp", None), P("sp", "tp")),
        check_vma=False,
    )
```

time: 54.9 us -> 52.4 us (0.954)
  the two profiles are of different devices: /device:TPU:6 before, /device:TPU:1 now
where the time goes in v5:
time: 52.4 us; the launch traced here: 52.2 us
  Pallas kernels  51.6 us (98%)
  between operations  0.64 us (1%)
    pallas_call x1, Pallas kernels, per_device(): pl.pallas_call(kernel, out_shape=results, in_specs=[pl.BlockSpec(memory_s...  50.2 us
    pallas_call x1, Pallas kernels, per_device(): pl.pallas_call(hand_over, out_shape=results, in_specs=[vmem] * 5, out_spe...  1.41 us

profile of v5, /device:TPU:1, one launch (start us, length us, event | category | flops | bytes accessed | tf_op | source)
XLA Modules:
  0.0 52.2 jit_solution(11884974689649647466)
XLA Ops:
  0.6 50.2 %shard_map.110 = (bf16[96,128]{1,0:T(8,128)(2,1)}, bf16[64,128]{1,0:T(8,128)(2,1)}, bf16[64,128]{1,0:T(8,128)(2,1)}, f32[32,128]{1,0:T(8,128)}, f32[8,128]{1,0:T(8,128)}) custom-call(bf16[96,128]{1,0:T(8,128)(2,1)} %bitcast.9, bf16[128,512]{1,0:T(8,128)(2,1)} %lat_hbm.1, bf16[32,128]{1,0:T(8,128)(2,1)} %bitcast.12, bf16[512,128]{1,0:T(8,128)(2,1)} %w_hbm.1, ...), custom_call_target="tpu_custom_call" | custom-call | tf_op jit(solution)/shard_map/pallas_call | solution.py:344
  50.8 1.4 %shard_map.111 = (bf16[96,128]{1,0:T(8,128)(2,1)}, bf16[64,128]{1,0:T(8,128)(2,1)}, bf16[64,128]{1,0:T(8,128)(2,1)}, f32[32,128]{1,0:T(8,128)}, f32[8,128]{1,0:T(8,128)}) custom-call(bf16[96,128]{1,0:T(8,128)(2,1)} %get-tuple-element.15.refs_0_, bf16[64,128]{1,0:T(8,128)(2,1)} %get-tuple-element.16.refs_1_, bf16[64,128]{1,0:T(8,128)(2,1)} %get-tuple-element.17.refs_2_, ...), custom_call_target="tpu_custom_call" | custom-call | tf_op jit(solution)/shard_map/pallas_call | solution.py:385

commit v6 on v5

--- a/solution.py
+++ b/solution.py
@@ -58,8 +58,8 @@
     q_hbm, lat_hbm, rot_hbm, w_hbm, lse_hbm, o_hbm, do_hbm,
     dq_ref, dk_ref, dv_ref, drot_ref, dw_ref,
     q_ref, lat_ref, w_ref, lse_ref, o_ref, do_ref,
-    qbuf, kvm, kvx, krot, kt, latt, mall, acc, dqp, dqb, dqr, dqs, dqz, dkvs, dkvr, halves, rots, rotr, rotx,
-    wsend, wrecv, wzs, wzr,
+    qbuf, kvm, kvx, krot, kt, latt, mall, acc, dqp, dqb, dqr, dqs, dqz, dkvs, dkvr, halves, rot_own, rots, rotr, rotx,
+    wsend, wnarrow, wrecv, wzs, wzr,
     isem, ssem, rsem,
 ):
     sp = lax.axis_index("sp")
@@ -127,9 +127,9 @@
     mine = pl.ds(PART * tp, PART)
     far = [
         [
+            copy(LAT + t - 1, latt.at[a, mine], latt.at[t, mine], device),
+            copy(K_ROT + t - 1, krot.at[a], krot.at[t], device),
             copy(K_FAR + t - 1, kvm.at[rows_of(a)], kvm.at[rows_of(t)], device),
-            copy(K_ROT + t - 1, krot.at[a], krot.at[t], device),
-            copy(LAT + t - 1, latt.at[a, mine], latt.at[t, mine], device),
         ]
         for t, a, device in ((1, 0, dev(4 * sign, 0)), (2, 0, dev(-4 * sign, 0)), (3, 1, dev(4 * sign, 0)))
     ]
@@ -138,7 +138,7 @@
         [copy(Q_Y + 3 * s + u - 1, qbuf.at[4 * s], qbuf.at[4 * s + u], dev(0, y_off[u])) for u in (1, 2, 3)]
         for s in range(4)
     ]
-    for c in far[0] + q_n + far[1] + q_y[0]:
+    for c in q_n + q_y[0] + far[0] + far[1]:
         c.start()
     for s in (1, 2, 3):
         q_n[s - 1].wait_recv()
@@ -168,6 +168,10 @@
         c.start()
     prepare(1)
     prepare(2)
+    far[2][0].wait_recv()
+    share_last = [copy(LAT_TP + 6 + k, latt.at[3, mine], latt.at[3, mine], others(k)) for k in range(1, NTP)]
+    for c in share_last:
+        c.start()
 
     def tile(s, first, count):
         m = mall[s]
@@ -208,11 +212,14 @@
         here = slice(ROWS * t, ROWS * (t + 1))
         main = acc[here, 0:128] * lane_scale
         hi = main.astype(BF16)
-        rots[t] = jnp.transpose(acc[here, 128:256])[0:ROPE] * SCALE
-        if t:
+        rot_part = jnp.transpose(acc[here, 128:256])[0:ROPE] * SCALE
+        if t == 0:
+            rot_own[...] = rot_part
+        else:
+            rots[t - 1] = rot_part.astype(BF16)
             dkvs[t - 1] = hi
             owner = dev(-f_off[t], 0)
-            drot.append(copy(DROT + t - 1, rots.at[t], rotr.at[t - 1], owner))
+            drot.append(copy(DROT + t - 1, rots.at[t - 1], rotr.at[t - 1], owner))
             drot[-1].start()
             dkv.append(copy(DKV + t - 1, dkvs.at[t - 1], dkvr.at[t - 1], owner))
             dkv[-1].start()
@@ -226,11 +233,8 @@
     wpart = dot(jnp.concatenate([latt[0], latt[1], latt[2]], axis=1), halves[0 : 3 * ROWS, :])
     wpart = wpart[:, 0:128] + wpart[:, 128:256]
 
-    for c in far[2]:
-        c.wait_recv()
-    share_last = [copy(LAT_TP + 6 + k, latt.at[3, mine], latt.at[3, mine], others(k)) for k in range(1, NTP)]
-    for c in share_last:
-        c.start()
+    for c in far[2][1:]:
+        c.wait_recv()
     prepare(3)
 
     def late(s, carry):
@@ -248,10 +252,11 @@
     more = dot(latt[3], halves[3 * ROWS : 4 * ROWS, :])
     wpart = (wpart + more[:, 0:128] + more[:, 128:256]).reshape(NZ, NY, 8, 128)
     for v in range(NY):
-        wsend[v] = wpart[:, v]
+        wsend[v] = wpart[:, v].reshape(NZ * 8, 128)
+    wnarrow[...] = wsend[...].astype(BF16)
     w_y = []
     for u in (1, 2, 3):
-        w_y.append(copy(W_Y + u - 1, wsend.at[(y + y_off[u] + NY) % NY], wrecv.at[u - 1], dev(0, y_off[u])))
+        w_y.append(copy(W_Y + u - 1, wnarrow.at[(y + y_off[u] + NY) % NY], wrecv.at[u - 1], dev(0, y_off[u])))
         w_y[-1].start()
 
     dq_y = [
@@ -271,25 +276,31 @@
 
     for c in w_y:
         c.wait_recv()
-    wzs[...] = wsend[y] + wrecv[0] + wrecv[1] + wrecv[2]
+    wsum = wsend[y]
+    for u in range(3):
+        wsum = wsum + wrecv[u].astype(F32)
+    wzs[...] = wsum.reshape(NZ, 8, 128)
     w_z = []
     for d in (8, 7, 9, 6, 10, 5, 11, 4, 12, 3, 13, 2, 14, 1, 15):
         w_z.append(copy(W_Z + d - 1, wzs.at[(z + d) % NZ], wzr.at[d - 1], dev(d, 0)))
         w_z[-1].start()
+
+    for c in drot:
+        c.wait_recv()
+    total = rot_own[...]
+    for t in range(3):
+        total = total + rotr[t].astype(F32)
+    rotx[tp] = total.astype(BF16)
+    rot = []
+    for k in range(1, NTP):
+        rot.append(copy(ROT + k - 1, rotx.at[tp], rotx.at[tp], others(k)))
+        rot[-1].start()
 
     dq_n = []
     for s in (3, 1, 2):
         dqs[s - 1] = dq_sum(s)
         dq_n.append(copy(DQ_N + s - 1, dqs.at[s - 1], dqz.at[s - 1], dev(-n_off[s], 0)))
         dq_n[-1].start()
-
-    for c in drot:
-        c.wait_recv()
-    rotx[tp] = rots[0] + rotr[0] + rotr[1] + rotr[2]
-    rot = []
-    for k in range(1, NTP):
-        rot.append(copy(ROT + k - 1, rotx.at[tp], rotx.at[tp], others(k)))
-        rot[-1].start()
 
     for c in dkv:
         c.wait_recv()
@@ -307,9 +318,9 @@
 
     for c in rot:
         c.wait_recv()
-    total = rotx[0]
+    total = rotx[0].astype(F32)
     for k in range(1, NTP):
-        total = total + rotx[k]
+        total = total + rotx[k].astype(F32)
     drot_ref[...] = total
 
     for c in w_z:
@@ -369,11 +380,13 @@
             pltpu.VMEM((3, ROWS, 128), BF16),
             pltpu.VMEM((3, ROWS, 128), BF16),
             pltpu.VMEM((4 * ROWS, 256), BF16),
-            pltpu.VMEM((4, ROPE, ROWS), F32),
-            pltpu.VMEM((3, ROPE, ROWS), F32),
-            pltpu.VMEM((NTP, ROPE, ROWS), F32),
-            pltpu.VMEM((NY, NZ, 8, 128), F32),
-            pltpu.VMEM((3, NZ, 8, 128), F32),
+            pltpu.VMEM((ROPE, ROWS), F32),
+            pltpu.VMEM((3, ROPE, ROWS), BF16),
+            pltpu.VMEM((3, ROPE, ROWS), BF16),
+            pltpu.VMEM((NTP, ROPE, ROWS), BF16),
+            pltpu.VMEM((NY, NZ * 8, 128), F32),
+            pltpu.VMEM((NY, NZ * 8, 128), BF16),
+            pltpu.VMEM((3, NZ * 8, 128), BF16),
             pltpu.VMEM((NZ, 8, 128), F32),
             pltpu.VMEM((NZ - 1, 8, 128), F32),
             pltpu.SemaphoreType.DMA((7,)),

time: 52.4 us -> 49.6 us (0.947)
  the two profiles are of different devices: /device:TPU:1 before, /device:TPU:6 now
where the time goes in v6:
time: 49.6 us; the launch traced here: 49.1 us
  Pallas kernels  48.5 us (98%)
  between operations  0.64 us (1%)
    pallas_call x1, Pallas kernels, per_device(): pl.pallas_call(kernel, out_shape=results, in_specs=[pl.BlockSpec(memory_s...  47.1 us
    pallas_call x1, Pallas kernels, per_device(): pl.pallas_call(hand_over, out_shape=results, in_specs=[vmem] * 5, out_spe...  1.41 us

profile of v6, /device:TPU:6, one launch (start us, length us, event | category | flops | bytes accessed | tf_op | source)
XLA Modules:
  0.0 49.1 jit_solution(17299870920109151445)
XLA Ops:
  0.6 47.1 %shard_map.110 = (bf16[96,128]{1,0:T(8,128)(2,1)}, bf16[64,128]{1,0:T(8,128)(2,1)}, bf16[64,128]{1,0:T(8,128)(2,1)}, f32[32,128]{1,0:T(8,128)}, f32[8,128]{1,0:T(8,128)}) custom-call(bf16[96,128]{1,0:T(8,128)(2,1)} %bitcast.9, bf16[128,512]{1,0:T(8,128)(2,1)} %lat_hbm.1, bf16[32,128]{1,0:T(8,128)(2,1)} %bitcast.12, bf16[512,128]{1,0:T(8,128)(2,1)} %w_hbm.1, ...), custom_call_target="tpu_custom_call" | custom-call | tf_op jit(solution)/shard_map/pallas_call | solution.py:355
  47.7 1.4 %shard_map.111 = (bf16[96,128]{1,0:T(8,128)(2,1)}, bf16[64,128]{1,0:T(8,128)(2,1)}, bf16[64,128]{1,0:T(8,128)(2,1)}, f32[32,128]{1,0:T(8,128)}, f32[8,128]{1,0:T(8,128)}) custom-call(bf16[96,128]{1,0:T(8,128)(2,1)} %get-tuple-element.15.refs_0_, bf16[64,128]{1,0:T(8,128)(2,1)} %get-tuple-element.16.refs_1_, bf16[64,128]{1,0:T(8,128)(2,1)} %get-tuple-element.17.refs_2_, ...), custom_call_target="tpu_custom_call" | custom-call | tf_op jit(solution)/shard_map/pallas_call | solution.py:398

commit v7 on v6

--- a/solution.py
+++ b/solution.py
@@ -59,7 +59,7 @@
     dq_ref, dk_ref, dv_ref, drot_ref, dw_ref,
     q_ref, lat_ref, w_ref, lse_ref, o_ref, do_ref,
     qbuf, kvm, kvx, krot, kt, latt, mall, acc, dqp, dqb, dqr, dqs, dqz, dkvs, dkvr, halves, rot_own, rots, rotr, rotx,
-    wsend, wnarrow, wrecv, wzs, wzr,
+    wsend, wnarrow, wrecv, wzs, wzb, wzr,
     isem, ssem, rsem,
 ):
     sp = lax.axis_index("sp")
@@ -226,12 +226,8 @@
         halves[here, 0:128] = hi
         halves[here, 128:256] = (main - hi.astype(F32)).astype(BF16)
 
-    for t in (1, 2, 0):
+    for t in (1, 2):
         finish(t)
-    for c in share:
-        c.wait_recv()
-    wpart = dot(jnp.concatenate([latt[0], latt[1], latt[2]], axis=1), halves[0 : 3 * ROWS, :])
-    wpart = wpart[:, 0:128] + wpart[:, 128:256]
 
     for c in far[2][1:]:
         c.wait_recv()
@@ -247,10 +243,11 @@
     lax.fori_loop(0, 4, late, 0)
 
     finish(3)
-    for c in share_last:
-        c.wait_recv()
-    more = dot(latt[3], halves[3 * ROWS : 4 * ROWS, :])
-    wpart = (wpart + more[:, 0:128] + more[:, 128:256]).reshape(NZ, NY, 8, 128)
+    finish(0)
+    for c in share + share_last:
+        c.wait_recv()
+    wpart = dot(jnp.concatenate([latt[0], latt[1], latt[2], latt[3]], axis=1), halves[...])
+    wpart = (wpart[:, 0:128] + wpart[:, 128:256]).reshape(NZ, NY, 8, 128)
     for v in range(NY):
         wsend[v] = wpart[:, v].reshape(NZ * 8, 128)
     wnarrow[...] = wsend[...].astype(BF16)
@@ -280,9 +277,10 @@
     for u in range(3):
         wsum = wsum + wrecv[u].astype(F32)
     wzs[...] = wsum.reshape(NZ, 8, 128)
+    wzb[...] = wzs[...].astype(BF16)
     w_z = []
     for d in (8, 7, 9, 6, 10, 5, 11, 4, 12, 3, 13, 2, 14, 1, 15):
-        w_z.append(copy(W_Z + d - 1, wzs.at[(z + d) % NZ], wzr.at[d - 1], dev(d, 0)))
+        w_z.append(copy(W_Z + d - 1, wzb.at[(z + d) % NZ], wzr.at[d - 1], dev(d, 0)))
         w_z[-1].start()
 
     for c in drot:
@@ -327,7 +325,7 @@
         c.wait_recv()
     wsum = wzs[z]
     for d in range(1, NZ):
-        wsum = wsum + wzr[d - 1]
+        wsum = wsum + wzr[d - 1].astype(F32)
     dw_ref[...] = wsum
 
     for c in q_n + share + share_last + dkv + drot + w_y + w_z + rot + dq_n:
@@ -388,7 +386,8 @@
             pltpu.VMEM((NY, NZ * 8, 128), BF16),
             pltpu.VMEM((3, NZ * 8, 128), BF16),
             pltpu.VMEM((NZ, 8, 128), F32),
-            pltpu.VMEM((NZ - 1, 8, 128), F32),
+            pltpu.VMEM((NZ, 8, 128), BF16),
+            pltpu.VMEM((NZ - 1, 8, 128), BF16),
             pltpu.SemaphoreType.DMA((7,)),
             pltpu.SemaphoreType.DMA((COPIES,)),
             pltpu.SemaphoreType.DMA((COPIES,)),

time: 49.6 us -> 49.3 us (level)
  no operation moved by 1% of the time
where the time goes in v7:
time: 49.3 us; the launch traced here: 48.9 us
  Pallas kernels  48.3 us (98%)
  between operations  0.64 us (1%)
    pallas_call x1, Pallas kernels, per_device(): pl.pallas_call(kernel, out_shape=results, in_specs=[pl.BlockSpec(memory_s...  46.8 us
    pallas_call x1, Pallas kernels, per_device(): pl.pallas_call(hand_over, out_shape=results, in_specs=[vmem] * 5, out_spe...  1.41 us

profile of v7, /device:TPU:6, one launch (start us, length us, event | category | flops | bytes accessed | tf_op | source)
XLA Modules:
  0.0 48.9 jit_solution(13343076340182326737)
XLA Ops:
  0.6 46.8 %shard_map.110 = (bf16[96,128]{1,0:T(8,128)(2,1)}, bf16[64,128]{1,0:T(8,128)(2,1)}, bf16[64,128]{1,0:T(8,128)(2,1)}, f32[32,128]{1,0:T(8,128)}, f32[8,128]{1,0:T(8,128)}) custom-call(bf16[96,128]{1,0:T(8,128)(2,1)} %bitcast.9, bf16[128,512]{1,0:T(8,128)(2,1)} %lat_hbm.1, bf16[32,128]{1,0:T(8,128)(2,1)} %bitcast.12, bf16[512,128]{1,0:T(8,128)(2,1)} %w_hbm.1, ...), custom_call_target="tpu_custom_call" | custom-call | tf_op jit(solution)/shard_map/pallas_call | solution.py:353
  47.5 1.4 %shard_map.111 = (bf16[96,128]{1,0:T(8,128)(2,1)}, bf16[64,128]{1,0:T(8,128)(2,1)}, bf16[64,128]{1,0:T(8,128)(2,1)}, f32[32,128]{1,0:T(8,128)}, f32[8,128]{1,0:T(8,128)}) custom-call(bf16[96,128]{1,0:T(8,128)(2,1)} %get-tuple-element.15.refs_0_, bf16[64,128]{1,0:T(8,128)(2,1)} %get-tuple-element.16.refs_1_, bf16[64,128]{1,0:T(8,128)(2,1)} %get-tuple-element.17.refs_2_, ...), custom_call_target="tpu_custom_call" | custom-call | tf_op jit(solution)/shard_map/pallas_call | solution.py:397

commit v8 on v7

--- a/solution.py
+++ b/solution.py
@@ -240,7 +240,8 @@
             dqb[4 * s + u] = total[:, 128 * u : 128 * u + 128].astype(BF16)
         return carry
 
-    lax.fori_loop(0, 4, late, 0)
+    for s in range(4):
+        late(s, 0)
 
     finish(3)
     finish(0)

time: 49.3 us -> 48.9 us (level)
  Pallas kernels: 48.3 us -> 47.7 us
    pallas_call x1, Pallas kernels: 46.8 us -> 46.3 us  [per_device(): pl.pallas_call(kernel, out_shape=results, in_specs=[pl.BlockSpec(memory_s...]
where the time goes in v8:
time: 48.9 us; the launch traced here: 48.4 us
  Pallas kernels  47.7 us (98%)
  between operations  0.64 us (1%)
    pallas_call x1, Pallas kernels, per_device(): pl.pallas_call(kernel, out_shape=results, in_specs=[pl.BlockSpec(memory_s...  46.3 us
    pallas_call x1, Pallas kernels, per_device(): pl.pallas_call(hand_over, out_shape=results, in_specs=[vmem] * 5, out_spe...  1.41 us

profile of v8, /device:TPU:6, one launch (start us, length us, event | category | flops | bytes accessed | tf_op | source)
XLA Modules:
  0.0 48.4 jit_solution(8077510097426580250)
XLA Ops:
  0.6 46.3 %shard_map.110 = (bf16[96,128]{1,0:T(8,128)(2,1)}, bf16[64,128]{1,0:T(8,128)(2,1)}, bf16[64,128]{1,0:T(8,128)(2,1)}, f32[32,128]{1,0:T(8,128)}, f32[8,128]{1,0:T(8,128)}) custom-call(bf16[96,128]{1,0:T(8,128)(2,1)} %bitcast.9, bf16[128,512]{1,0:T(8,128)(2,1)} %lat_hbm.1, bf16[32,128]{1,0:T(8,128)(2,1)} %bitcast.12, bf16[512,128]{1,0:T(8,128)(2,1)} %w_hbm.1, ...), custom_call_target="tpu_custom_call" | custom-call | tf_op jit(solution)/shard_map/pallas_call | solution.py:354
  46.9 1.4 %shard_map.111 = (bf16[96,128]{1,0:T(8,128)(2,1)}, bf16[64,128]{1,0:T(8,128)(2,1)}, bf16[64,128]{1,0:T(8,128)(2,1)}, f32[32,128]{1,0:T(8,128)}, f32[8,128]{1,0:T(8,128)}) custom-call(bf16[96,128]{1,0:T(8,128)(2,1)} %get-tuple-element.15.refs_0_, bf16[64,128]{1,0:T(8,128)(2,1)} %get-tuple-element.16.refs_1_, bf16[64,128]{1,0:T(8,128)(2,1)} %get-tuple-element.17.refs_2_, ...), custom_call_target="tpu_custom_call" | custom-call | tf_op jit(solution)/shard_map/pallas_call | solution.py:398
